TPU v7x, 32 devices: a whole 2x2x4 slice. The times are simulated.
32 devices in a mesh: grp: 2 (over x), ep: 16 (over z, y, core).
Axes of the slice: x: 2, y: 2, z: 4, core: 2. Of those that a mesh axis runs over, the one named last changes fastest.
Arguments:
- tokens: bfloat16 [4096, 2048], P(('grp', 'ep')), parts along dimension 0, may hold values from -6 to 6
- norm_gain: float32 [2048], replicated, may hold values from 0.1 to 1.9
- expert_ids: int32 [4096, 2], P(('grp', 'ep')), parts along dimension 0, may hold values from 0 to 3, as said below
- mix_weights: float32 [4096, 2], P(('grp', 'ep')), parts along dimension 0, may hold values from 0.2 to 1
- gate_weight: bfloat16 [2048, 28672], P(None, 'ep'), may hold values from -0.125 to 0.125
- up_weight: bfloat16 [2048, 28672], P(None, 'ep'), may hold values from -0.125 to 0.125
- down_weight: bfloat16 [28672, 2048], P('ep'), may hold values from -0.0625 to 0.0625
Outputs:
- mixed: bfloat16 [4096, 2048], P(('grp', 'ep')), parts along dimension 0
There are 2 independent parts, one for each index of `grp`. A program takes and returns all parts, laid end to end along the dimension named above; an argument that names none is the same for every part. Nothing has to cross between parts.
Inputs may be any that keep to these rules, and one draw needn't show every extreme that they name: `expert_ids`: each token names 2 different experts. In the rows of one device no expert is named by more than 80 rows, and in every draw each expert is named by exactly 80 rows of some device.
All inputs are finite; a program needn't handle non-finite values.
Results may differ from a plain program's by a relative error of at most 0.008.
Values may be sent and summed in bfloat16 or wider, within the bound.
No kernel may reach another device: no remote copies, remote signals or barrier semaphores. Data moves between devices by JAX's collectives and lax.ppermute only.
A program may use at most 128 MiB of HBM per device.

v0:
```python
import functools

import jax
import jax.numpy as jnp
from jax import lax
from jax.experimental import pallas as pl
from jax.experimental.pallas import tpu as pltpu
from jax.sharding import PartitionSpec as P


TOP = 2
SPLIT = 4
FF_TILE = 256
OUT_TILE = 512
VMEM = pl.BlockSpec(memory_space=pltpu.VMEM)
SMEM = pl.BlockSpec(memory_space=pltpu.SMEM)
HBM = pl.BlockSpec(memory_space=pltpu.HBM)


def places(ids, expert, capacity):
    tokens = ids.shape[1]
    named = ids[0:1] == expert
    for pick in range(1, TOP):
        named = named | (ids[pick : pick + 1] == expert)
    rows = lax.broadcasted_iota(jnp.int32, (tokens, tokens), 0)
    cols = lax.broadcasted_iota(jnp.int32, (tokens, tokens), 1)
    earlier = (rows < cols).astype(jnp.float32).astype(jnp.bfloat16)
    flags = jnp.broadcast_to(named.astype(jnp.float32), (8, tokens)).astype(jnp.bfloat16)
    slot = jnp.dot(flags, earlier, preferred_element_type=jnp.float32)[0:1].astype(jnp.int32)
    slot = jnp.where(named, slot, -1)
    places_of = lax.broadcasted_iota(jnp.int32, (capacity, tokens), 0)
    return (places_of == slot).astype(jnp.float32).astype(jnp.bfloat16)


def dispatch_kernel(experts, capacity, mine, ids, tokens, gain, *outs):
    values = tokens[...].astype(jnp.float32)
    scale = lax.rsqrt(jnp.mean(values * values, axis=-1, keepdims=True) + 1e-06)
    normed = (values * scale * gain[...]).astype(jnp.bfloat16)
    for shift in range(experts):
        onehot = places(ids[...], lax.rem(mine[0] + shift, experts), capacity)
        outs[shift][...] = jnp.dot(onehot, normed, preferred_element_type=jnp.float32).astype(
            jnp.bfloat16
        )


def combine_kernel(experts, capacity, mine, ids, mix, *refs):
    rets, out = refs[:experts], refs[experts]
    tokens = ids.shape[1]
    total = jnp.zeros(out.shape, jnp.float32)
    for shift in range(experts):
        expert = lax.rem(mine[0] + shift, experts)
        onehot = places(ids[...], expert, capacity)
        weight = jnp.zeros((1, tokens), jnp.float32)
        for pick in range(TOP):
            weight = weight + jnp.where(ids[pick : pick + 1] == expert, mix[pick : pick + 1], 0.0)
        column = jnp.transpose(jnp.broadcast_to(weight, (tokens, tokens)))[:, 0:1]
        rows = lax.dot_general(
            onehot, rets[shift][...], (((0,), (0,)), ((), ())), preferred_element_type=jnp.float32
        )
        total = total + column * rows
    out[...] = total.astype(out.dtype)


def load_kernel(*refs):
    count = len(refs) // 2
    copies = [
        pltpu.make_async_copy(refs[i], refs[count + i], refs[-1].at[i]) for i in range(count)
    ]
    for copy in copies:
        copy.start()
    for copy in copies:
        copy.wait()


def ffn_kernel(*refs):
    xs, (gate_w, up_w, down_w), outs, (inputs, hidden) = (
        refs[:SPLIT],
        refs[SPLIT : SPLIT + 3],
        refs[SPLIT + 3 : 2 * SPLIT + 3],
        refs[2 * SPLIT + 3 :],
    )
    capacity = xs[0].shape[0]
    for i, block in enumerate(xs):
        inputs[i * capacity : (i + 1) * capacity] = block[...]
    for start in range(0, gate_w.shape[1], FF_TILE):
        cols = pl.ds(start, FF_TILE)
        gate = jnp.dot(inputs[...], gate_w[:, cols], preferred_element_type=jnp.float32)
        upper = jnp.dot(inputs[...], up_w[:, cols], preferred_element_type=jnp.float32)
        hidden[:, cols] = (gate / (1.0 + jnp.exp(-gate)) * upper).astype(jnp.bfloat16)
    for start in range(0, down_w.shape[1], OUT_TILE):
        cols = pl.ds(start, OUT_TILE)
        result = jnp.dot(hidden[...], down_w[:, cols], preferred_element_type=jnp.float32)
        for i, out in enumerate(outs):
            out[:, cols] = result[i * capacity : (i + 1) * capacity].astype(out.dtype)


def shifts(experts):
    return [0] + sorted(range(1, experts), key=lambda d: (min(d, experts - d), d))


def local(tokens, norm_gain, expert_ids, mix_weights, gate_weight, up_weight, down_weight):
    n_dev = lax.axis_size("ep")
    experts = n_dev // SPLIT
    tok_rows, width = tokens.shape
    ff = gate_weight.shape[1]
    capacity = SPLIT * ((tok_rows * TOP * SPLIT * 5 // (4 * n_dev) + SPLIT - 1) // SPLIT)
    mine = (lax.axis_index("ep") // SPLIT).astype(jnp.int32).reshape(1)
    ids = expert_ids.T
    mix = mix_weights.T
    block = jax.ShapeDtypeStruct((capacity, width), jnp.bfloat16)

    def across(array, shift):
        pairs = [(i, (i // SPLIT + shift) % experts * SPLIT + i % SPLIT) for i in range(n_dev)]
        return lax.ppermute(array, "ep", pairs)

    def inside(array, flip):
        return lax.ppermute(array, "ep", [(i, i ^ flip) for i in range(n_dev)])

    def add(*parts):
        return sum(part.astype(jnp.float32) for part in parts).astype(jnp.bfloat16)

    sent = pl.pallas_call(
        functools.partial(dispatch_kernel, experts, capacity),
        out_shape=[block] * experts,
        in_specs=[SMEM, VMEM, VMEM, VMEM],
        out_specs=[VMEM] * experts,
        compiler_params=pltpu.CompilerParams(vmem_limit_bytes=8 * 2**20),
        cost_estimate=pl.CostEstimate(
            flops=2 * experts * capacity * tok_rows * width,
            bytes_accessed=4 * tok_rows * width,
            transcendentals=0,
        ),
        name="route",
    )(mine, ids, tokens, norm_gain.reshape(1, width))

    weights = (gate_weight, up_weight, down_weight)
    weights = pl.pallas_call(
        load_kernel,
        out_shape=[pltpu.VMEM(w.shape, w.dtype) for w in weights],
        in_specs=[HBM] * len(weights),
        out_specs=[VMEM] * len(weights),
        scratch_shapes=[pltpu.SemaphoreType.DMA((len(weights),))],
        compiler_params=pltpu.CompilerParams(vmem_limit_bytes=2**20),
        cost_estimate=pl.CostEstimate(
            flops=6 * 2**30, bytes_accessed=6 * width * ff, transcendentals=0
        ),
        name="fetch",
    )(*weights)

    rows = SPLIT * capacity
    ffn = pl.pallas_call(
        ffn_kernel,
        out_shape=[block] * SPLIT,
        in_specs=[VMEM] * (SPLIT + 3),
        out_specs=[VMEM] * SPLIT,
        scratch_shapes=[
            pltpu.VMEM((rows, width), jnp.bfloat16),
            pltpu.VMEM((rows, ff), jnp.bfloat16),
        ],
        compiler_params=pltpu.CompilerParams(vmem_limit_bytes=8 * 2**20),
        cost_estimate=pl.CostEstimate(
            flops=6 * rows * width * ff, bytes_accessed=6 * width * ff, transcendentals=rows * ff
        ),
        name="experts",
    )

    order = shifts(experts)
    arrived = {d: across(sent[d], d) if d else sent[d] for d in order}
    rets = [None] * experts
    for d in order:
        own = arrived[d]
        side = inside(own, 2)
        twin = inside(own, 1)
        twin_side = inside(side, 1)
        part, part_side, part_twin, part_twin_side = ffn(own, side, twin, twin_side, *weights)
        got_side = inside(part_twin_side, 1)
        got = inside(part_twin, 1)
        sum_side = add(part_side, got_side)
        got_far = inside(sum_side, 2)
        total = add(part, got, got_far)
        rets[d] = across(total, experts - d) if d else total

    return pl.pallas_call(
        functools.partial(combine_kernel, experts, capacity),
        out_shape=jax.ShapeDtypeStruct((tok_rows, width), jnp.bfloat16),
        in_specs=[SMEM, VMEM, VMEM] + [VMEM] * experts,
        out_specs=VMEM,
        compiler_params=pltpu.CompilerParams(vmem_limit_bytes=8 * 2**20),
        name="combine",
    )(mine, ids, mix, *rets)


def solution(mesh):
    in_specs = (
        P(("grp", "ep"), None),
        P(),
        P(("grp", "ep"), None),
        P(("grp", "ep"), None),
        P(None, "ep"),
        P(None, "ep"),
        P("ep", None),
    )
    out_specs = P(("grp", "ep"), None)
    return jax.shard_map(local, mesh=mesh, in_specs=in_specs, out_specs=out_specs, check_vma=False)
```

profile of v0, /device:TPU:24, one launch (start us, length us, event | category | flops | bytes accessed | tf_op | source)
XLA Modules:
  0.0 133.0 jit_solution(9368984993001590994)
XLA Ops:
  0.7 1.0 copy-done.6
  2.4 1.1 route.1
  4.0 1.5 %collective-permute-start = (bf16[80,2048]{1,0:T(8,128)(2,1)S(1)}, bf16[80,2048]{1,0:T(8,128)(2,1)S(1)}, u32[]{:S(2)}, u32[]{:S(2)}) collective-permute-start(bf16[80,2048]{1,0:T(8,128)(2,1)S(1)} %get-tuple-element.28.refs_0_), channel_id=1, source_target_pairs={{0,2},{1,3},{2,0},{3,1},{4,6},{5,7},{6,4},{7,5},{8,10},{9,11},{10,... | collective-permute-start | bytes 983048 | tf_op jit(solution)/shard_map/ppermute | solution.py:117
  5.9 3.0 %collective-permute-start.6 = (bf16[80,2048]{1,0:T(8,128)(2,1)S(1)}, bf16[80,2048]{1,0:T(8,128)(2,1)S(1)}, u32[]{:S(2)}, u32[]{:S(2)}) collective-permute-start(bf16[80,2048]{1,0:T(8,128)(2,1)S(1)} %get-tuple-element.36), channel_id=1, source_target_pairs={{0,4},{1,5},{2,6},{3,7},{4,8},{5,9},{6,10},{7,11},{8,12},{9,13},{1... | collective-permute-start | bytes 983048 | tf_op jit(solution)/shard_map/ppermute | solution.py:114
  8.9 7.2 %collective-permute-done.22.refs_0_ = bf16[80,2048]{1,0:T(8,128)(2,1)S(1)} collective-permute-done((bf16[80,2048]{1,0:T(8,128)(2,1)S(1)}, bf16[80,2048]{1,0:T(8,128)(2,1)S(1)}, u32[]{:S(2)}, u32[]{:S(2)}) %collective-permute-start.22) | collective-permute-done | bytes 327712 | tf_op jit(solution)/shard_map/ppermute | solution.py:114
  16.1 1.5 %collective-permute-start.23 = (bf16[80,2048]{1,0:T(8,128)(2,1)S(1)}, bf16[80,2048]{1,0:T(8,128)(2,1)S(1)}, u32[]{:S(2)}, u32[]{:S(2)}) collective-permute-start(bf16[80,2048]{1,0:T(8,128)(2,1)S(1)} %collective-permute-done.22.refs_0_), channel_id=1, source_target_pairs={{0,2},{1,3},{2,0},{3,1},{4,6},{5,7},{6,4},{7,5},{8,10},{9,11},{10,... | collective-permute-start | bytes 983048 | tf_op jit(solution)/shard_map/ppermute | solution.py:117
  17.6 3.1 %copy-done.3 = bf16[2048,1792]{1,0:T(8,128)(2,1)S(1)} copy-done((bf16[2048,1792]{1,0:T(8,128)(2,1)S(1)}, bf16[2048,1792]{1,0:T(8,128)(2,1)}, u32[]{:S(2)}) %copy-start.3) | copy-done | bytes 7340056
  20.7 3.1 %copy-done.4 = bf16[2048,1792]{1,0:T(8,128)(2,1)S(1)} copy-done((bf16[2048,1792]{1,0:T(8,128)(2,1)S(1)}, bf16[2048,1792]{1,0:T(8,128)(2,1)}, u32[]{:S(2)}) %copy-start.4) | copy-done | bytes 7340056
  23.8 3.1 %copy-done.5 = bf16[1792,2048]{1,0:T(8,128)(2,1)S(1)} copy-done((bf16[1792,2048]{1,0:T(8,128)(2,1)S(1)}, bf16[1792,2048]{1,0:T(8,128)(2,1)}, u32[]{:S(2)}) %copy-start.5) | copy-done | bytes 7340056
  26.9 1.5 %fetch.1 = (bf16[2048,1792]{1,0:T(8,128)(2,1)S(1)}, bf16[2048,1792]{1,0:T(8,128)(2,1)S(1)}, bf16[1792,2048]{1,0:T(8,128)(2,1)S(1)}) custom-call(bf16[2048,1792]{1,0:T(8,128)(2,1)S(1)} %copy-done.3, bf16[2048,1792]{1,0:T(8,128)(2,1)S(1)} %copy-done.4, bf16[1792,2048]{1,0:T(8,128)(2,1)S(1)} %copy-done.5), custom_call_target="tpu_custom_call" | custom-call | flops 6442450944 | bytes 22020096 | tf_op jit(solution)/shard_map/fetch/pallas_call | solution.py:137
  29.0 1.5 %collective-permute-start.15 = (bf16[80,2048]{1,0:T(8,128)(2,1)S(1)}, bf16[80,2048]{1,0:T(8,128)(2,1)S(1)}, u32[]{:S(2)}, u32[]{:S(2)}) collective-permute-start(bf16[80,2048]{1,0:T(8,128)(2,1)S(1)} %collective-permute-done.14.refs_0_), channel_id=1, source_target_pairs={{0,2},{1,3},{2,0},{3,1},{4,6},{5,7},{6,4},{7,5},{8,10},{9,11},{10,... | collective-permute-start | bytes 983048 | tf_op jit(solution)/shard_map/ppermute | solution.py:117
  31.3 7.3 %experts.4 = (bf16[80,2048]{1,0:T(8,128)(2,1)S(1)}, bf16[80,2048]{1,0:T(8,128)(2,1)S(1)}, bf16[80,2048]{1,0:T(8,128)(2,1)S(1)}, bf16[80,2048]{1,0:T(8,128)(2,1)S(1)}) custom-call(bf16[80,2048]{1,0:T(8,128)(2,1)S(1)} %get-tuple-element.28.refs_0_, bf16[80,2048]{1,0:T(8,128)(2,1)S(1)} %collective-permute-done.refs_1_, ...), custom_call_target="tpu_custom_call" | custom-call | flops 7046430720 | bytes 22020096 | tf_op jit(solution)/shard_map/experts/pallas_call | solution.py:175
  40.1 7.3 %experts.7 = (bf16[80,2048]{1,0:T(8,128)(2,1)S(1)}, bf16[80,2048]{1,0:T(8,128)(2,1)S(1)}, bf16[80,2048]{1,0:T(8,128)(2,1)S(1)}, bf16[80,2048]{1,0:T(8,128)(2,1)S(1)}) custom-call(bf16[80,2048]{1,0:T(8,128)(2,1)S(1)} %collective-permute-done.22.refs_0_, bf16[80,2048]{1,0:T(8,128)(2,1)S(1)} %collective-permute-done.23.refs_1_, ...), custom_call_target="tpu_custom_call" | custom-call | flops 7046430720 | bytes 22020096 | tf_op jit(solution)/shard_map/experts/pallas_call | solution.py:175
  48.0 7.5 %experts.6 = (bf16[80,2048]{1,0:T(8,128)(2,1)S(1)}, bf16[80,2048]{1,0:T(8,128)(2,1)S(1)}, bf16[80,2048]{1,0:T(8,128)(2,1)S(1)}, bf16[80,2048]{1,0:T(8,128)(2,1)S(1)}) custom-call(bf16[80,2048]{1,0:T(8,128)(2,1)S(1)} %collective-permute-done.14.refs_0_, bf16[80,2048]{1,0:T(8,128)(2,1)S(1)} %collective-permute-done.15.refs_1_, ...), custom_call_target="tpu_custom_call" | custom-call | flops 7046430720 | bytes 22020096 | tf_op jit(solution)/shard_map/experts/pallas_call | solution.py:175
  56.1 7.3 %experts.5 = (bf16[80,2048]{1,0:T(8,128)(2,1)S(1)}, bf16[80,2048]{1,0:T(8,128)(2,1)S(1)}, bf16[80,2048]{1,0:T(8,128)(2,1)S(1)}, bf16[80,2048]{1,0:T(8,128)(2,1)S(1)}) custom-call(bf16[80,2048]{1,0:T(8,128)(2,1)S(1)} %collective-permute-done.6.refs_0_, bf16[80,2048]{1,0:T(8,128)(2,1)S(1)} %collective-permute-done.7.refs_1_, ...), custom_call_target="tpu_custom_call" | custom-call | flops 7046430720 | bytes 22020096 | tf_op jit(solution)/shard_map/experts/pallas_call | solution.py:175
  65.7 1.5 %collective-permute-start.28 = (bf16[80,2048]{1,0:T(8,128)(2,1)S(1)}, bf16[80,2048]{1,0:T(8,128)(2,1)S(1)}, u32[]{:S(2)}, u32[]{:S(2)}) collective-permute-start(bf16[80,2048]{1,0:T(8,128)(2,1)S(1)} %add_convert_fusion.1), channel_id=1, source_target_pairs={{0,2},{1,3},{2,0},{3,1},{4,6},{5,7},{6,4},{7,5},{8,10},{9,11},{10,... | collective-permute-start | bytes 983048 | tf_op jit(solution)/shard_map/ppermute | solution.py:117
  67.9 8.4 %collective-permute-done.28 = bf16[80,2048]{1,0:T(8,128)(2,1)S(1)} collective-permute-done((bf16[80,2048]{1,0:T(8,128)(2,1)S(1)}, bf16[80,2048]{1,0:T(8,128)(2,1)S(1)}, u32[]{:S(2)}, u32[]{:S(2)}) %collective-permute-start.28) | collective-permute-done | bytes 327712 | tf_op jit(solution)/shard_map/ppermute | solution.py:117
  76.3 1.5 %collective-permute-start.20 = (bf16[80,2048]{1,0:T(8,128)(2,1)S(1)}, bf16[80,2048]{1,0:T(8,128)(2,1)S(1)}, u32[]{:S(2)}, u32[]{:S(2)}) collective-permute-start(bf16[80,2048]{1,0:T(8,128)(2,1)S(1)} %add_convert_fusion.3), channel_id=1, source_target_pairs={{0,2},{1,3},{2,0},{3,1},{4,6},{5,7},{6,4},{7,5},{8,10},{9,11},{10,... | collective-permute-start | bytes 983048 | tf_op jit(solution)/shard_map/ppermute | solution.py:117
  78.5 11.8 %collective-permute-done.20 = bf16[80,2048]{1,0:T(8,128)(2,1)S(1)} collective-permute-done((bf16[80,2048]{1,0:T(8,128)(2,1)S(1)}, bf16[80,2048]{1,0:T(8,128)(2,1)S(1)}, u32[]{:S(2)}, u32[]{:S(2)}) %collective-permute-start.20) | collective-permute-done | bytes 327712 | tf_op jit(solution)/shard_map/ppermute | solution.py:117
  90.4 6.3 %collective-permute-start.29 = (bf16[80,2048]{1,0:T(8,128)(2,1)S(1)}, bf16[80,2048]{1,0:T(8,128)(2,1)S(1)}, u32[]{:S(2)}, u32[]{:S(2)}) collective-permute-start(bf16[80,2048]{1,0:T(8,128)(2,1)S(1)} %add_convert_fusion), channel_id=1, source_target_pairs={{0,4},{1,5},{2,6},{3,7},{4,8},{5,9},{6,10},{7,11},{8,12},{9,13},{1... | collective-permute-start | bytes 983048 | tf_op jit(solution)/shard_map/ppermute | solution.py:114
  96.8 6.2 %collective-permute-start.21 = (bf16[80,2048]{1,0:T(8,128)(2,1)S(1)}, bf16[80,2048]{1,0:T(8,128)(2,1)S(1)}, u32[]{:S(2)}, u32[]{:S(2)}) collective-permute-start(bf16[80,2048]{1,0:T(8,128)(2,1)S(1)} %add_convert_fusion.2), channel_id=1, source_target_pairs={{0,8},{1,9},{2,10},{3,11},{4,12},{5,13},{6,14},{7,15},{8,0},{9,1},... | collective-permute-start | bytes 983048 | tf_op jit(solution)/shard_map/ppermute | solution.py:114
  103.1 2.1 %collective-permute-start.13 = (bf16[80,2048]{1,0:T(8,128)(2,1)S(1)}, bf16[80,2048]{1,0:T(8,128)(2,1)S(1)}, u32[]{:S(2)}, u32[]{:S(2)}) collective-permute-start(bf16[80,2048]{1,0:T(8,128)(2,1)S(1)} %add_convert_fusion.4), channel_id=1, source_target_pairs={{0,12},{1,13},{2,14},{3,15},{4,0},{5,1},{6,2},{7,3},{8,4},{9,5},{1... | collective-permute-start | bytes 983048 | tf_op jit(solution)/shard_map/ppermute | solution.py:114
  105.3 25.2 %collective-permute-done.21.refs_2_ = bf16[80,2048]{1,0:T(8,128)(2,1)S(1)} collective-permute-done((bf16[80,2048]{1,0:T(8,128)(2,1)S(1)}, bf16[80,2048]{1,0:T(8,128)(2,1)S(1)}, u32[]{:S(2)}, u32[]{:S(2)}) %collective-permute-start.21) | collective-permute-done | bytes 327712 | tf_op jit(solution)/shard_map/ppermute | solution.py:114
  130.5 2.5 %combine.1 = bf16[128,2048]{1,0:T(8,128)(2,1)} custom-call(s32[1]{0:T(128)} %bitcast.mine, s32[2,128]{1,0:T(2,128)S(1)} %bitcast.5, f32[2,128]{1,0:T(2,128)S(1)} %bitcast.6, bf16[80,2048]{1,0:T(8,128)(2,1)S(1)} %add_convert_fusion.6.refs_0_, bf16[80,2048]{1,0:T(8,128)(2,1)S(1)} %collective-permute-done.13.refs_1_, ...), custom_call_target="tpu_custom_call" | custom-call | tf_op jit(solution)/shard_map/combine/pallas_call | solution.py:183
  (67 shorter events, 10.4 us)
Async XLA Ops:
  3.5 12.6 %collective-permute-start.22 = (bf16[80,2048]{1,0:T(8,128)(2,1)S(1)}, bf16[80,2048]{1,0:T(8,128)(2,1)S(1)}, u32[]{:S(2)}, u32[]{:S(2)}) collective-permute-start(bf16[80,2048]{1,0:T(8,128)(2,1)S(1)} %get-tuple-element.46), channel_id=1, source_target_pairs={{0,12},{1,13},{2,14},{3,15},{4,0},{5,1},{6,2},{7,3},{8,4},{9,5},{1... | collective-permute-start | bytes 983048 | tf_op jit(solution)/shard_map/ppermute | solution.py:114
  4.0 13.6 %collective-permute-start = (bf16[80,2048]{1,0:T(8,128)(2,1)S(1)}, bf16[80,2048]{1,0:T(8,128)(2,1)S(1)}, u32[]{:S(2)}, u32[]{:S(2)}) collective-permute-start(bf16[80,2048]{1,0:T(8,128)(2,1)S(1)} %get-tuple-element.28.refs_0_), channel_id=1, source_target_pairs={{0,2},{1,3},{2,0},{3,1},{4,6},{5,7},{6,4},{7,5},{8,10},{9,11},{10,... | collective-permute-start | bytes 983048 | tf_op jit(solution)/shard_map/ppermute | solution.py:117
  5.5 25.0 %collective-permute-start.1 = (bf16[80,2048]{1,0:T(8,128)(2,1)S(1)}, bf16[80,2048]{1,0:T(8,128)(2,1)S(1)}, u32[]{:S(2)}, u32[]{:S(2)}) collective-permute-start(bf16[80,2048]{1,0:T(8,128)(2,1)S(1)} %get-tuple-element.28.refs_0_), channel_id=1, source_target_pairs={{0,1},{1,0},{2,3},{3,2},{4,5},{5,4},{6,7},{7,6},{8,9},{9,8},{10,11... | collective-permute-start | bytes 983048 | tf_op jit(solution)/shard_map/ppermute | solution.py:117
  5.6 23.4 %collective-permute-start.14 = (bf16[80,2048]{1,0:T(8,128)(2,1)S(1)}, bf16[80,2048]{1,0:T(8,128)(2,1)S(1)}, u32[]{:S(2)}, u32[]{:S(2)}) collective-permute-start(bf16[80,2048]{1,0:T(8,128)(2,1)S(1)} %get-tuple-element.41), channel_id=1, source_target_pairs={{0,8},{1,9},{2,10},{3,11},{4,12},{5,13},{6,14},{7,15},{8,0},{9,1},... | collective-permute-start | bytes 983048 | tf_op jit(solution)/shard_map/ppermute | solution.py:114
  5.9 23.1 %collective-permute-start.6 = (bf16[80,2048]{1,0:T(8,128)(2,1)S(1)}, bf16[80,2048]{1,0:T(8,128)(2,1)S(1)}, u32[]{:S(2)}, u32[]{:S(2)}) collective-permute-start(bf16[80,2048]{1,0:T(8,128)(2,1)S(1)} %get-tuple-element.36), channel_id=1, source_target_pairs={{0,4},{1,5},{2,6},{3,7},{4,8},{5,9},{6,10},{7,11},{8,12},{9,13},{1... | collective-permute-start | bytes 983048 | tf_op jit(solution)/shard_map/ppermute | solution.py:114
  16.1 14.6 %collective-permute-start.23 = (bf16[80,2048]{1,0:T(8,128)(2,1)S(1)}, bf16[80,2048]{1,0:T(8,128)(2,1)S(1)}, u32[]{:S(2)}, u32[]{:S(2)}) collective-permute-start(bf16[80,2048]{1,0:T(8,128)(2,1)S(1)} %collective-permute-done.22.refs_0_), channel_id=1, source_target_pairs={{0,2},{1,3},{2,0},{3,1},{4,6},{5,7},{6,4},{7,5},{8,10},{9,11},{10,... | collective-permute-start | bytes 983048 | tf_op jit(solution)/shard_map/ppermute | solution.py:117
  17.6 13.6 %collective-permute-start.2 = (bf16[80,2048]{1,0:T(8,128)(2,1)S(1)}, bf16[80,2048]{1,0:T(8,128)(2,1)S(1)}, u32[]{:S(2)}, u32[]{:S(2)}) collective-permute-start(bf16[80,2048]{1,0:T(8,128)(2,1)S(1)} %collective-permute-done.refs_1_), channel_id=1, source_target_pairs={{0,1},{1,0},{2,3},{3,2},{4,5},{5,4},{6,7},{7,6},{8,9},{9,8},{10,11... | collective-permute-start | bytes 983048 | tf_op jit(solution)/shard_map/ppermute | solution.py:117
  29.0 10.6 %collective-permute-start.15 = (bf16[80,2048]{1,0:T(8,128)(2,1)S(1)}, bf16[80,2048]{1,0:T(8,128)(2,1)S(1)}, u32[]{:S(2)}, u32[]{:S(2)}) collective-permute-start(bf16[80,2048]{1,0:T(8,128)(2,1)S(1)} %collective-permute-done.14.refs_0_), channel_id=1, source_target_pairs={{0,2},{1,3},{2,0},{3,1},{4,6},{5,7},{6,4},{7,5},{8,10},{9,11},{10,... | collective-permute-start | bytes 983048 | tf_op jit(solution)/shard_map/ppermute | solution.py:117
  30.5 16.9 %collective-permute-start.16 = (bf16[80,2048]{1,0:T(8,128)(2,1)S(1)}, bf16[80,2048]{1,0:T(8,128)(2,1)S(1)}, u32[]{:S(2)}, u32[]{:S(2)}) collective-permute-start(bf16[80,2048]{1,0:T(8,128)(2,1)S(1)} %collective-permute-done.14.refs_0_), channel_id=1, source_target_pairs={{0,1},{1,0},{2,3},{3,2},{4,5},{5,4},{6,7},{7,6},{8,9},{9,8},{10,11... | collective-permute-start | bytes 983048 | tf_op jit(solution)/shard_map/ppermute | solution.py:117
  30.7 16.8 %collective-permute-start.7 = (bf16[80,2048]{1,0:T(8,128)(2,1)S(1)}, bf16[80,2048]{1,0:T(8,128)(2,1)S(1)}, u32[]{:S(2)}, u32[]{:S(2)}) collective-permute-start(bf16[80,2048]{1,0:T(8,128)(2,1)S(1)} %collective-permute-done.6.refs_0_), channel_id=1, source_target_pairs={{0,2},{1,3},{2,0},{3,1},{4,6},{5,7},{6,4},{7,5},{8,10},{9,11},{10,... | collective-permute-start | bytes 983048 | tf_op jit(solution)/shard_map/ppermute | solution.py:117
  38.6 17.0 %collective-permute-start.8 = (bf16[80,2048]{1,0:T(8,128)(2,1)S(1)}, bf16[80,2048]{1,0:T(8,128)(2,1)S(1)}, u32[]{:S(2)}, u32[]{:S(2)}) collective-permute-start(bf16[80,2048]{1,0:T(8,128)(2,1)S(1)} %collective-permute-done.6.refs_0_), channel_id=1, source_target_pairs={{0,1},{1,0},{2,3},{3,2},{4,5},{5,4},{6,7},{7,6},{8,9},{9,8},{10,11... | collective-permute-start | bytes 983048 | tf_op jit(solution)/shard_map/ppermute | solution.py:117
  39.6 23.9 %collective-permute-start.4 = (bf16[80,2048]{1,0:T(8,128)(2,1)S(1)}, bf16[80,2048]{1,0:T(8,128)(2,1)S(1)}, u32[]{:S(2)}, u32[]{:S(2)}) collective-permute-start(bf16[80,2048]{1,0:T(8,128)(2,1)S(1)} %get-tuple-element.35), channel_id=1, source_target_pairs={{0,1},{1,0},{2,3},{3,2},{4,5},{5,4},{6,7},{7,6},{8,9},{9,8},{10,11... | collective-permute-start | bytes 983048 | tf_op jit(solution)/shard_map/ppermute | solution.py:117
  47.4 57.8 %collective-permute-start.3 = (bf16[80,2048]{1,0:T(8,128)(2,1)S(1)}, bf16[80,2048]{1,0:T(8,128)(2,1)S(1)}, u32[]{:S(2)}, u32[]{:S(2)}) collective-permute-start(bf16[80,2048]{1,0:T(8,128)(2,1)S(1)} %get-tuple-element.33), channel_id=1, source_target_pairs={{0,1},{1,0},{2,3},{3,2},{4,5},{5,4},{6,7},{7,6},{8,9},{9,8},{10,11... | collective-permute-start | bytes 983048 | tf_op jit(solution)/shard_map/ppermute | solution.py:117
  48.0 16.1 %collective-permute-start.27 = (bf16[80,2048]{1,0:T(8,128)(2,1)S(1)}, bf16[80,2048]{1,0:T(8,128)(2,1)S(1)}, u32[]{:S(2)}, u32[]{:S(2)}) collective-permute-start(bf16[80,2048]{1,0:T(8,128)(2,1)S(1)} %get-tuple-element.50), channel_id=1, source_target_pairs={{0,1},{1,0},{2,3},{3,2},{4,5},{5,4},{6,7},{7,6},{8,9},{9,8},{10,11... | collective-permute-start | bytes 983048 | tf_op jit(solution)/shard_map/ppermute | solution.py:117
  55.5 11.8 %collective-permute-start.26 = (bf16[80,2048]{1,0:T(8,128)(2,1)S(1)}, bf16[80,2048]{1,0:T(8,128)(2,1)S(1)}, u32[]{:S(2)}, u32[]{:S(2)}) collective-permute-start(bf16[80,2048]{1,0:T(8,128)(2,1)S(1)} %get-tuple-element.48), channel_id=1, source_target_pairs={{0,1},{1,0},{2,3},{3,2},{4,5},{5,4},{6,7},{7,6},{8,9},{9,8},{10,11... | collective-permute-start | bytes 983048 | tf_op jit(solution)/shard_map/ppermute | solution.py:117
  63.4 14.5 %collective-permute-start.18 = (bf16[80,2048]{1,0:T(8,128)(2,1)S(1)}, bf16[80,2048]{1,0:T(8,128)(2,1)S(1)}, u32[]{:S(2)}, u32[]{:S(2)}) collective-permute-start(bf16[80,2048]{1,0:T(8,128)(2,1)S(1)} %get-tuple-element.43), channel_id=1, source_target_pairs={{0,1},{1,0},{2,3},{3,2},{4,5},{5,4},{6,7},{7,6},{8,9},{9,8},{10,11... | collective-permute-start | bytes 983048 | tf_op jit(solution)/shard_map/ppermute | solution.py:117
  64.3 32.5 %collective-permute-start.10 = (bf16[80,2048]{1,0:T(8,128)(2,1)S(1)}, bf16[80,2048]{1,0:T(8,128)(2,1)S(1)}, u32[]{:S(2)}, u32[]{:S(2)}) collective-permute-start(bf16[80,2048]{1,0:T(8,128)(2,1)S(1)} %get-tuple-element.38), channel_id=1, source_target_pairs={{0,1},{1,0},{2,3},{3,2},{4,5},{5,4},{6,7},{7,6},{8,9},{9,8},{10,11... | collective-permute-start | bytes 983048 | tf_op jit(solution)/shard_map/ppermute | solution.py:117
  65.7 10.6 %collective-permute-start.28 = (bf16[80,2048]{1,0:T(8,128)(2,1)S(1)}, bf16[80,2048]{1,0:T(8,128)(2,1)S(1)}, u32[]{:S(2)}, u32[]{:S(2)}) collective-permute-start(bf16[80,2048]{1,0:T(8,128)(2,1)S(1)} %add_convert_fusion.1), channel_id=1, source_target_pairs={{0,2},{1,3},{2,0},{3,1},{4,6},{5,7},{6,4},{7,5},{8,10},{9,11},{10,... | collective-permute-start | bytes 983048 | tf_op jit(solution)/shard_map/ppermute | solution.py:117
  67.3 37.9 %collective-permute-start.5 = (bf16[80,2048]{1,0:T(8,128)(2,1)S(1)}, bf16[80,2048]{1,0:T(8,128)(2,1)S(1)}, u32[]{:S(2)}, u32[]{:S(2)}) collective-permute-start(bf16[80,2048]{1,0:T(8,128)(2,1)S(1)} %add_convert_fusion.7), channel_id=1, source_target_pairs={{0,2},{1,3},{2,0},{3,1},{4,6},{5,7},{6,4},{7,5},{8,10},{9,11},{10,... | collective-permute-start | bytes 983048 | tf_op jit(solution)/shard_map/ppermute | solution.py:117
  76.3 14.0 %collective-permute-start.20 = (bf16[80,2048]{1,0:T(8,128)(2,1)S(1)}, bf16[80,2048]{1,0:T(8,128)(2,1)S(1)}, u32[]{:S(2)}, u32[]{:S(2)}) collective-permute-start(bf16[80,2048]{1,0:T(8,128)(2,1)S(1)} %add_convert_fusion.3), channel_id=1, source_target_pairs={{0,2},{1,3},{2,0},{3,1},{4,6},{5,7},{6,4},{7,5},{8,10},{9,11},{10,... | collective-permute-start | bytes 983048 | tf_op jit(solution)/shard_map/ppermute | solution.py:117
  78.0 25.0 %collective-permute-start.12 = (bf16[80,2048]{1,0:T(8,128)(2,1)S(1)}, bf16[80,2048]{1,0:T(8,128)(2,1)S(1)}, u32[]{:S(2)}, u32[]{:S(2)}) collective-permute-start(bf16[80,2048]{1,0:T(8,128)(2,1)S(1)} %add_convert_fusion.5), channel_id=1, source_target_pairs={{0,2},{1,3},{2,0},{3,1},{4,6},{5,7},{6,4},{7,5},{8,10},{9,11},{10,... | collective-permute-start | bytes 983048 | tf_op jit(solution)/shard_map/ppermute | solution.py:117
  90.4 15.0 %collective-permute-start.29 = (bf16[80,2048]{1,0:T(8,128)(2,1)S(1)}, bf16[80,2048]{1,0:T(8,128)(2,1)S(1)}, u32[]{:S(2)}, u32[]{:S(2)}) collective-permute-start(bf16[80,2048]{1,0:T(8,128)(2,1)S(1)} %add_convert_fusion), channel_id=1, source_target_pairs={{0,4},{1,5},{2,6},{3,7},{4,8},{5,9},{6,10},{7,11},{8,12},{9,13},{1... | collective-permute-start | bytes 983048 | tf_op jit(solution)/shard_map/ppermute | solution.py:114
  96.8 33.7 %collective-permute-start.21 = (bf16[80,2048]{1,0:T(8,128)(2,1)S(1)}, bf16[80,2048]{1,0:T(8,128)(2,1)S(1)}, u32[]{:S(2)}, u32[]{:S(2)}) collective-permute-start(bf16[80,2048]{1,0:T(8,128)(2,1)S(1)} %add_convert_fusion.2), channel_id=1, source_target_pairs={{0,8},{1,9},{2,10},{3,11},{4,12},{5,13},{6,14},{7,15},{8,0},{9,1},... | collective-permute-start | bytes 983048 | tf_op jit(solution)/shard_map/ppermute | solution.py:114
  103.1 27.4 %collective-permute-start.13 = (bf16[80,2048]{1,0:T(8,128)(2,1)S(1)}, bf16[80,2048]{1,0:T(8,128)(2,1)S(1)}, u32[]{:S(2)}, u32[]{:S(2)}) collective-permute-start(bf16[80,2048]{1,0:T(8,128)(2,1)S(1)} %add_convert_fusion.4), channel_id=1, source_target_pairs={{0,12},{1,13},{2,14},{3,15},{4,0},{5,1},{6,2},{7,3},{8,4},{9,5},{1... | collective-permute-start | bytes 983048 | tf_op jit(solution)/shard_map/ppermute | solution.py:114
  (14 other events, 190.7 us)
where the time goes:
time: 133 us
  waiting for transfers between devices  54.5 us (41%)
  Pallas kernels  34.4 us (26%)
  starting transfers between devices  31.4 us (24%)
  local copies, waits for them, and re-layouts  11.7 us (9%)
    ppermute x6, waiting for transfers between devices, across(): return lax.ppermute(array, 'ep', pairs)  32.9 us
    pallas_call x4, Pallas kernels, local(): ffn(own, side, twin, twin_side, *weights)  29.3 us
    ppermute x24, waiting for transfers between devices, inside(): return lax.ppermute(array, 'ep', [(i, i ^ flip) for i in range(n_dev)])  21.6 us
    ppermute x6, starting transfers between devices, across(): return lax.ppermute(array, 'ep', pairs)  18.5 us
    ppermute x24, starting transfers between devices, inside(): return lax.ppermute(array, 'ep', [(i, i ^ flip) for i in range(n_dev)])  12.9 us
    unnamed x16, local copies, waits for them, and re-layouts  11.7 us
  transfers between devices with their start and end apart: 30, of which 7 were waited for; matrix products, arithmetic and copies ran while one was open for 1% of the time, Pallas kernels for 23%

commit v1 on v0

v1 whole, which is shorter than its diff:
```python
import functools

import jax
import jax.numpy as jnp
from jax import lax
from jax.experimental import pallas as pl
from jax.experimental.pallas import tpu as pltpu
from jax.sharding import PartitionSpec as P


TOP = 2
SPLIT = 4
FF_TILE = 256
OUT_TILE = 512
VMEM = pl.BlockSpec(memory_space=pltpu.VMEM)
SMEM = pl.BlockSpec(memory_space=pltpu.SMEM)
EARLY = 1
LATE = (1, 0)
HBM = pl.BlockSpec(memory_space=pltpu.HBM)


def places(ids, expert, capacity):
    tokens = ids.shape[1]
    named = ids[0:1] == expert
    for pick in range(1, TOP):
        named = named | (ids[pick : pick + 1] == expert)
    rows = lax.broadcasted_iota(jnp.int32, (tokens, tokens), 0)
    cols = lax.broadcasted_iota(jnp.int32, (tokens, tokens), 1)
    earlier = (rows < cols).astype(jnp.float32).astype(jnp.bfloat16)
    flags = jnp.broadcast_to(named.astype(jnp.float32), (8, tokens)).astype(jnp.bfloat16)
    slot = jnp.dot(flags, earlier, preferred_element_type=jnp.float32)[0:1].astype(jnp.int32)
    slot = jnp.where(named, slot, -1)
    places_of = lax.broadcasted_iota(jnp.int32, (capacity, tokens), 0)
    return (places_of == slot).astype(jnp.float32).astype(jnp.bfloat16)


def dispatch_kernel(experts, capacity, mine, *refs):
    sources, outs, held, sem = refs[:3], refs[3 : 3 + experts], refs[3 + experts : -1], refs[-1]
    copies = [
        pltpu.make_async_copy(src, dst, sem.at[i]) for i, (src, dst) in enumerate(zip(sources, held))
    ]
    for copy in copies:
        copy.start()
    ids, tokens, gain = held
    copies[0].wait()
    onehots = [places(ids[...], lax.rem(mine[0] + d, experts), capacity) for d in range(experts)]
    for copy in copies[1:]:
        copy.wait()
    values = tokens[...].astype(jnp.float32)
    scale = lax.rsqrt(jnp.mean(values * values, axis=-1, keepdims=True) + 1e-06)
    normed = (values * scale * gain[...]).astype(jnp.bfloat16)
    for onehot, out in zip(onehots, outs):
        out[...] = jnp.dot(onehot, normed, preferred_element_type=jnp.float32).astype(jnp.bfloat16)


def combine_kernel(experts, capacity, chosen, last, mine, ids, mix, *refs):
    rets, refs = refs[: len(chosen)], refs[len(chosen) :]
    total = refs[0][...] if last else None
    out = refs[-1]
    tokens = ids.shape[1]
    for shift, ret in zip(chosen, rets):
        expert = lax.rem(mine[0] + shift, experts)
        onehot = places(ids[...], expert, capacity)
        weight = jnp.zeros((1, tokens), jnp.float32)
        for pick in range(TOP):
            weight = weight + jnp.where(ids[pick : pick + 1] == expert, mix[pick : pick + 1], 0.0)
        column = jnp.transpose(jnp.broadcast_to(weight, (tokens, tokens)))[:, 0:1]
        rows = lax.dot_general(
            onehot, ret[...], (((0,), (0,)), ((), ())), preferred_element_type=jnp.float32
        )
        total = column * rows if total is None else total + column * rows
    out[...] = total.astype(out.dtype)


def ffn_body(xs, weights, outs, inputs, hidden, ready):
    gate_w, up_w, down_w = weights
    capacity = xs[0].shape[0]
    for i, block in enumerate(xs):
        inputs[i * capacity : (i + 1) * capacity] = block[...]
    for start in range(0, gate_w.shape[1], FF_TILE):
        ready()
        cols = pl.ds(start, FF_TILE)
        gate = jnp.dot(inputs[...], gate_w[:, cols], preferred_element_type=jnp.float32)
        upper = jnp.dot(inputs[...], up_w[:, cols], preferred_element_type=jnp.float32)
        hidden[:, cols] = (gate / (1.0 + jnp.exp(-gate)) * upper).astype(jnp.bfloat16)
    for start in range(0, down_w.shape[1], OUT_TILE):
        ready()
        cols = pl.ds(start, OUT_TILE)
        result = jnp.dot(hidden[...], down_w[:, cols], preferred_element_type=jnp.float32)
        for i, out in enumerate(outs):
            out[:, cols] = result[i * capacity : (i + 1) * capacity].astype(out.dtype)


def ffn_kernel(count, *refs):
    xs, weights, outs = refs[:count], refs[count : count + 3], refs[count + 3 : 2 * count + 3]
    ffn_body(xs, weights, outs, refs[-2], refs[-1], lambda: None)


def first_ffn_kernel(count, *refs):
    xs, stored, refs = refs[:count], refs[count : count + 3], refs[count + 3 :]
    outs, weights, (inputs, hidden, sem) = refs[:count], refs[count : count + 3], refs[count + 3 :]
    groups = []
    for start in range(0, weights[0].shape[1], FF_TILE):
        groups.append([(k, pl.ds(start, FF_TILE)) for k in range(2)])
    for start in range(0, weights[2].shape[1], OUT_TILE):
        groups.append([(2, pl.ds(start, OUT_TILE))])
    copies, n = [], 0
    for group in groups:
        made = []
        for k, cols in group:
            made.append(
                pltpu.make_async_copy(stored[k].at[:, cols], weights[k].at[:, cols], sem.at[n])
            )
            n += 1
        copies.append(made)
    for made in copies:
        for copy in made:
            copy.start()
    left = iter(copies)

    def ready():
        for copy in next(left):
            copy.wait()

    ffn_body(xs, weights, outs, inputs, hidden, ready)


def shifts(experts):
    return [0] + sorted(range(1, experts), key=lambda d: (min(d, experts - d), d))


def local(tokens, norm_gain, expert_ids, mix_weights, gate_weight, up_weight, down_weight):
    n_dev = lax.axis_size("ep")
    experts = n_dev // SPLIT
    tok_rows, width = tokens.shape
    ff = gate_weight.shape[1]
    capacity = SPLIT * ((tok_rows * TOP * SPLIT * 5 // (4 * n_dev) + SPLIT - 1) // SPLIT)
    mine = (lax.axis_index("ep") // SPLIT).astype(jnp.int32).reshape(1)
    ids = expert_ids.T
    mix = mix_weights.T
    block = jax.ShapeDtypeStruct((capacity, width), jnp.bfloat16)

    def across(array, shift):
        pairs = [(i, (i // SPLIT + shift) % experts * SPLIT + i % SPLIT) for i in range(n_dev)]
        return lax.ppermute(array, "ep", pairs)

    def inside(array, flip):
        return lax.ppermute(array, "ep", [(i, i ^ flip) for i in range(n_dev)])

    def add(*parts):
        return sum(part.astype(jnp.float32) for part in parts).astype(jnp.bfloat16)

    inputs = (ids, tokens, norm_gain.reshape(1, width))
    sent = pl.pallas_call(
        functools.partial(dispatch_kernel, experts, capacity),
        out_shape=[block] * experts,
        in_specs=[SMEM, HBM, HBM, HBM],
        out_specs=[VMEM] * experts,
        scratch_shapes=[pltpu.VMEM(array.shape, array.dtype) for array in inputs]
        + [pltpu.SemaphoreType.DMA((len(inputs),))],
        compiler_params=pltpu.CompilerParams(vmem_limit_bytes=8 * 2**20),
        cost_estimate=pl.CostEstimate(
            flops=2 * experts * capacity * tok_rows * width,
            bytes_accessed=4 * tok_rows * width,
            transcendentals=0,
        ),
        name="route",
    )(mine, *(pltpu.with_memory_space_constraint(array, pltpu.HBM) for array in inputs))

    weights = (gate_weight, up_weight, down_weight)
    half = SPLIT // 2
    rows = half * capacity
    tiles = 2 * (ff // FF_TILE) + width // OUT_TILE
    scratch = [
        pltpu.VMEM((rows, width), jnp.bfloat16),
        pltpu.VMEM((rows, ff), jnp.bfloat16),
    ]
    shared = dict(
        compiler_params=pltpu.CompilerParams(vmem_limit_bytes=8 * 2**20),
        cost_estimate=pl.CostEstimate(
            flops=6 * rows * width * ff, bytes_accessed=6 * width * ff, transcendentals=rows * ff
        ),
        name="experts",
    )
    ffn = pl.pallas_call(
        functools.partial(ffn_kernel, half),
        out_shape=[block] * half,
        in_specs=[VMEM] * (half + 3),
        out_specs=[VMEM] * half,
        scratch_shapes=scratch,
        **shared,
    )
    first_ffn = pl.pallas_call(
        functools.partial(first_ffn_kernel, half),
        out_shape=[block] * half + [pltpu.VMEM(w.shape, w.dtype) for w in weights],
        in_specs=[VMEM] * half + [HBM] * 3,
        out_specs=[VMEM] * (half + 3),
        scratch_shapes=scratch + [pltpu.SemaphoreType.DMA((tiles,))],
        **shared,
    )

    order = shifts(experts)
    rets = [None] * experts
    for d in order:
        if d == 0:
            own = sent[0]
            side = inside(own, 2)
        elif d == EARLY:
            own = across(sent[d], d)
            side = across(inside(sent[d], 2), d)
        else:
            own = across(sent[d], d)
            side = inside(own, 2)
        twin = inside(own, 1)
        twin_side = inside(side, 1)
        if d == 0:
            kept = (pltpu.with_memory_space_constraint(w, pltpu.HBM) for w in weights)
            part, part_twin, *weights = first_ffn(own, twin, *kept)
        else:
            part, part_twin = ffn(own, twin, *weights)
        part_side, part_twin_side = ffn(side, twin_side, *weights)
        got_side = inside(part_twin_side, 1)
        got = inside(part_twin, 1)
        sum_side = add(part_side, got_side)
        got_far = inside(sum_side, 2)
        total = add(part, got, got_far)
        rets[d] = across(total, experts - d) if d else total

    def combine(chosen, dtype, *before):
        return pl.pallas_call(
            functools.partial(combine_kernel, experts, capacity, chosen, bool(before)),
            out_shape=jax.ShapeDtypeStruct((tok_rows, width), dtype),
            in_specs=[SMEM] + [VMEM] * (2 + len(chosen) + len(before)),
            out_specs=VMEM,
            compiler_params=pltpu.CompilerParams(vmem_limit_bytes=8 * 2**20),
            cost_estimate=pl.CostEstimate(
                flops=2 * len(chosen) * capacity * tok_rows * width,
                bytes_accessed=8 * tok_rows * width,
                transcendentals=0,
            ),
            name="combine",
        )(mine, ids, mix, *(rets[d] for d in chosen), *before)

    late = LATE if experts == 4 else tuple(order[-1:])
    early = combine(tuple(d for d in order if d not in late), jnp.float32)
    return combine(late, jnp.bfloat16, early)


def solution(mesh):
    in_specs = (
        P(("grp", "ep"), None),
        P(),
        P(("grp", "ep"), None),
        P(("grp", "ep"), None),
        P(None, "ep"),
        P(None, "ep"),
        P("ep", None),
    )
    out_specs = P(("grp", "ep"), None)
    return jax.shard_map(local, mesh=mesh, in_specs=in_specs, out_specs=out_specs, check_vma=False)
```

time: 133 us -> 133 us (level)
  the two profiles are of different devices: /device:TPU:24 before, /device:TPU:0 now
where the time goes in v1:
time: 133 us
  waiting for transfers between devices  59 us (44%)
  Pallas kernels  39.2 us (29%)
  starting transfers between devices  33.2 us (25%)
    ppermute x7, waiting for transfers between devices, across(): return lax.ppermute(array, 'ep', pairs)  33 us
    ppermute x24, waiting for transfers between devices, inside(): return lax.ppermute(array, 'ep', [(i, i ^ flip) for i in range(n_dev)])  26.1 us
    ppermute x7, starting transfers between devices, across(): return lax.ppermute(array, 'ep', pairs)  19.1 us
    pallas_call x4, Pallas kernels, local(): part_side, part_twin_side = ffn(side, twin_side, *weights)  15.4 us
    ppermute x24, starting transfers between devices, inside(): return lax.ppermute(array, 'ep', [(i, i ^ flip) for i in range(n_dev)])  14.1 us
    pallas_call x3, Pallas kernels, local(): part, part_twin = ffn(own, twin, *weights)  11.3 us
    pallas_call x1, Pallas kernels, local(): part, part_twin, *weights = first_ffn(own, twin, *kept)  8.26 us
  transfers between devices with their start and end apart: 31, of which 10 were waited for; matrix products, arithmetic and copies ran while one was open for 1% of the time, Pallas kernels for 27%

profile of v1, /device:TPU:0, one launch (start us, length us, event | category | flops | bytes accessed | tf_op | source)
XLA Modules:
  0.0 132.5 jit_solution(17392980500407319584)
XLA Ops:
  0.0 1.8 %route.1 = (bf16[80,2048]{1,0:T(8,128)(2,1)S(1)}, bf16[80,2048]{1,0:T(8,128)(2,1)S(1)}, bf16[80,2048]{1,0:T(8,128)(2,1)S(1)}, bf16[80,2048]{1,0:T(8,128)(2,1)S(1)}) custom-call(s32[1]{0:T(128)} %bitcast.mine, s32[2,128]{1,0:T(2,128)} %bitcast.4, bf16[128,2048]{1,0:T(8,128)(2,1)} %refs_1_.1, f32[1,2048]{1,0:T(1,128)} %bitcast.9), custom_call_target="tpu_custom_call" | custom-call | flops 167772160 | bytes 1048576 | tf_op jit(solution)/shard_map/route/pallas_call | solution.py:154
  2.3 2.6 %collective-permute-start = (bf16[80,2048]{1,0:T(8,128)(2,1)S(1)}, bf16[80,2048]{1,0:T(8,128)(2,1)S(1)}, u32[]{:S(2)}, u32[]{:S(2)}) collective-permute-start(bf16[80,2048]{1,0:T(8,128)(2,1)S(1)} %get-tuple-element.28), channel_id=1, source_target_pairs={{0,4},{1,5},{2,6},{3,7},{4,8},{5,9},{6,10},{7,11},{8,12},{9,13},{1... | collective-permute-start | bytes 983048 | tf_op jit(solution)/shard_map/ppermute | solution.py:145
  7.0 2.1 %collective-permute-start.15 = (bf16[80,2048]{1,0:T(8,128)(2,1)S(1)}, bf16[80,2048]{1,0:T(8,128)(2,1)S(1)}, u32[]{:S(2)}, u32[]{:S(2)}) collective-permute-start(bf16[80,2048]{1,0:T(8,128)(2,1)S(1)} %get-tuple-element.41), channel_id=1, source_target_pairs={{0,12},{1,13},{2,14},{3,15},{4,0},{5,1},{6,2},{7,3},{8,4},{9,5},{1... | collective-permute-start | bytes 983048 | tf_op jit(solution)/shard_map/ppermute | solution.py:145
  10.0 5.6 %collective-permute-done.refs_0_ = bf16[80,2048]{1,0:T(8,128)(2,1)S(1)} collective-permute-done((bf16[80,2048]{1,0:T(8,128)(2,1)S(1)}, bf16[80,2048]{1,0:T(8,128)(2,1)S(1)}, u32[]{:S(2)}, u32[]{:S(2)}) %collective-permute-start) | collective-permute-done | bytes 327712 | tf_op jit(solution)/shard_map/ppermute | solution.py:145
  15.6 8.3 %experts.8 = (bf16[80,2048]{1,0:T(8,128)(2,1)S(1)}, bf16[80,2048]{1,0:T(8,128)(2,1)S(1)}, bf16[2048,1792]{1,0:T(8,128)(2,1)S(1)}, bf16[2048,1792]{1,0:T(8,128)(2,1)S(1)}, bf16[1792,2048]{1,0:T(8,128)(2,1)S(1)}) custom-call(bf16[80,2048]{1,0:T(8,128)(2,1)S(1)} %get-tuple-element.29.refs_0_, bf16[80,2048]{1,0:T(8,128)(2,1)S(1)} %collective-permute-done.2.refs_1_, ...), custom_call_target="tpu_custom_call" | custom-call | flops 3523215360 | bytes 22020096 | tf_op jit(solution)/shard_map/experts/pallas_call | solution.py:218
  24.5 1.7 %collective-permute-start.18 = (bf16[80,2048]{1,0:T(8,128)(2,1)S(1)}, bf16[80,2048]{1,0:T(8,128)(2,1)S(1)}, u32[]{:S(2)}, u32[]{:S(2)}) collective-permute-start(bf16[80,2048]{1,0:T(8,128)(2,1)S(1)} %collective-permute-done.15.refs_0_), channel_id=1, source_target_pairs={{0,2},{1,3},{2,0},{3,1},{4,6},{5,7},{6,4},{7,5},{8,10},{9,11},{10,... | collective-permute-start | bytes 983048 | tf_op jit(solution)/shard_map/ppermute | solution.py:148
  26.3 3.8 %experts.9 = (bf16[80,2048]{1,0:T(8,128)(2,1)S(1)}, bf16[80,2048]{1,0:T(8,128)(2,1)S(1)}) custom-call(bf16[80,2048]{1,0:T(8,128)(2,1)S(1)} %collective-permute-done.refs_0_, bf16[80,2048]{1,0:T(8,128)(2,1)S(1)} %collective-permute-done.1.refs_1_, bf16[2048,1792]{1,0:T(8,128)(2,1)S(1)} %get-tuple-element.30.refs_2_, ...), custom_call_target="tpu_custom_call" | custom-call | flops 3523215360 | bytes 22020096 | tf_op jit(solution)/shard_map/experts/pallas_call | solution.py:220
  30.1 6.3 %collective-permute-done.23.refs_0_ = bf16[80,2048]{1,0:T(8,128)(2,1)S(1)} collective-permute-done((bf16[80,2048]{1,0:T(8,128)(2,1)S(1)}, bf16[80,2048]{1,0:T(8,128)(2,1)S(1)}, u32[]{:S(2)}, u32[]{:S(2)}) %collective-permute-start.23) | collective-permute-done | bytes 327712 | tf_op jit(solution)/shard_map/ppermute | solution.py:145
  36.4 1.5 %collective-permute-start.26 = (bf16[80,2048]{1,0:T(8,128)(2,1)S(1)}, bf16[80,2048]{1,0:T(8,128)(2,1)S(1)}, u32[]{:S(2)}, u32[]{:S(2)}) collective-permute-start(bf16[80,2048]{1,0:T(8,128)(2,1)S(1)} %collective-permute-done.23.refs_0_), channel_id=1, source_target_pairs={{0,2},{1,3},{2,0},{3,1},{4,6},{5,7},{6,4},{7,5},{8,10},{9,11},{10,... | collective-permute-start | bytes 983048 | tf_op jit(solution)/shard_map/ppermute | solution.py:148
  37.9 3.8 %experts.11 = (bf16[80,2048]{1,0:T(8,128)(2,1)S(1)}, bf16[80,2048]{1,0:T(8,128)(2,1)S(1)}) custom-call(bf16[80,2048]{1,0:T(8,128)(2,1)S(1)} %collective-permute-done.11.refs_0_, bf16[80,2048]{1,0:T(8,128)(2,1)S(1)} %collective-permute-done.12.refs_1_, bf16[2048,1792]{1,0:T(8,128)(2,1)S(1)} %get-tuple-element.30.refs_2_, ...), custom_call_target="tpu_custom_call" | custom-call | flops 3523215360 | bytes 22020096 | tf_op jit(solution)/shard_map/experts/pallas_call | solution.py:221
  42.0 5.6 %collective-permute-start.5 = (bf16[80,2048]{1,0:T(8,128)(2,1)S(1)}, bf16[80,2048]{1,0:T(8,128)(2,1)S(1)}, u32[]{:S(2)}, u32[]{:S(2)}) collective-permute-start(bf16[80,2048]{1,0:T(8,128)(2,1)S(1)} %collective-permute-done.4), channel_id=1, source_target_pairs={{0,4},{1,5},{2,6},{3,7},{4,8},{5,9},{6,10},{7,11},{8,12},{9,13},{1... | collective-permute-start | bytes 983048 | tf_op jit(solution)/shard_map/ppermute | solution.py:145
  47.6 3.8 %experts.12 = (bf16[80,2048]{1,0:T(8,128)(2,1)S(1)}, bf16[80,2048]{1,0:T(8,128)(2,1)S(1)}) custom-call(bf16[80,2048]{1,0:T(8,128)(2,1)S(1)} %collective-permute-done.15.refs_0_, bf16[80,2048]{1,0:T(8,128)(2,1)S(1)} %collective-permute-done.16.refs_1_, bf16[2048,1792]{1,0:T(8,128)(2,1)S(1)} %get-tuple-element.30.refs_2_, ...), custom_call_target="tpu_custom_call" | custom-call | flops 3523215360 | bytes 22020096 | tf_op jit(solution)/shard_map/experts/pallas_call | solution.py:220
  51.5 3.8 %experts.14 = (bf16[80,2048]{1,0:T(8,128)(2,1)S(1)}, bf16[80,2048]{1,0:T(8,128)(2,1)S(1)}) custom-call(bf16[80,2048]{1,0:T(8,128)(2,1)S(1)} %collective-permute-done.23.refs_0_, bf16[80,2048]{1,0:T(8,128)(2,1)S(1)} %collective-permute-done.24.refs_1_, bf16[2048,1792]{1,0:T(8,128)(2,1)S(1)} %get-tuple-element.30.refs_2_, ...), custom_call_target="tpu_custom_call" | custom-call | flops 3523215360 | bytes 22020096 | tf_op jit(solution)/shard_map/experts/pallas_call | solution.py:220
  58.0 3.8 %experts.10 = (bf16[80,2048]{1,0:T(8,128)(2,1)S(1)}, bf16[80,2048]{1,0:T(8,128)(2,1)S(1)}) custom-call(bf16[80,2048]{1,0:T(8,128)(2,1)S(1)} %collective-permute-done.5.refs_0_, bf16[80,2048]{1,0:T(8,128)(2,1)S(1)} %collective-permute-done.6.refs_1_, bf16[2048,1792]{1,0:T(8,128)(2,1)S(1)} %get-tuple-element.30.refs_2_, ...), custom_call_target="tpu_custom_call" | custom-call | flops 3523215360 | bytes 22020096 | tf_op jit(solution)/shard_map/experts/pallas_call | solution.py:221
  62.3 4.0 %experts.13 = (bf16[80,2048]{1,0:T(8,128)(2,1)S(1)}, bf16[80,2048]{1,0:T(8,128)(2,1)S(1)}) custom-call(bf16[80,2048]{1,0:T(8,128)(2,1)S(1)} %collective-permute-done.18.refs_0_, bf16[80,2048]{1,0:T(8,128)(2,1)S(1)} %collective-permute-done.19.refs_1_, bf16[2048,1792]{1,0:T(8,128)(2,1)S(1)} %get-tuple-element.30.refs_2_, ...), custom_call_target="tpu_custom_call" | custom-call | flops 3523215360 | bytes 22020096 | tf_op jit(solution)/shard_map/experts/pallas_call | solution.py:221
  66.6 3.8 %experts.15 = (bf16[80,2048]{1,0:T(8,128)(2,1)S(1)}, bf16[80,2048]{1,0:T(8,128)(2,1)S(1)}) custom-call(bf16[80,2048]{1,0:T(8,128)(2,1)S(1)} %collective-permute-done.26.refs_0_, bf16[80,2048]{1,0:T(8,128)(2,1)S(1)} %collective-permute-done.27.refs_1_, bf16[2048,1792]{1,0:T(8,128)(2,1)S(1)} %get-tuple-element.30.refs_2_, ...), custom_call_target="tpu_custom_call" | custom-call | flops 3523215360 | bytes 22020096 | tf_op jit(solution)/shard_map/experts/pallas_call | solution.py:221
  75.9 8.4 %collective-permute-done.8 = bf16[80,2048]{1,0:T(8,128)(2,1)S(1)} collective-permute-done((bf16[80,2048]{1,0:T(8,128)(2,1)S(1)}, bf16[80,2048]{1,0:T(8,128)(2,1)S(1)}, u32[]{:S(2)}, u32[]{:S(2)}) %collective-permute-start.8) | collective-permute-done | bytes 327712 | tf_op jit(solution)/shard_map/ppermute | solution.py:148
  86.5 11.8 %collective-permute-done.21 = bf16[80,2048]{1,0:T(8,128)(2,1)S(1)} collective-permute-done((bf16[80,2048]{1,0:T(8,128)(2,1)S(1)}, bf16[80,2048]{1,0:T(8,128)(2,1)S(1)}, u32[]{:S(2)}, u32[]{:S(2)}) %collective-permute-start.21) | collective-permute-done | bytes 327712 | tf_op jit(solution)/shard_map/ppermute | solution.py:148
  98.4 3.8 %collective-permute-start.9 = (bf16[80,2048]{1,0:T(8,128)(2,1)S(1)}, bf16[80,2048]{1,0:T(8,128)(2,1)S(1)}, u32[]{:S(2)}, u32[]{:S(2)}) collective-permute-start(bf16[80,2048]{1,0:T(8,128)(2,1)S(1)} %add_convert_fusion.6), channel_id=1, source_target_pairs={{0,12},{1,13},{2,14},{3,15},{4,0},{5,1},{6,2},{7,3},{8,4},{9,5},{1... | collective-permute-start | bytes 983048 | tf_op jit(solution)/shard_map/ppermute | solution.py:145
  102.4 2.4 %collective-permute-done.29 = bf16[80,2048]{1,0:T(8,128)(2,1)S(1)} collective-permute-done((bf16[80,2048]{1,0:T(8,128)(2,1)S(1)}, bf16[80,2048]{1,0:T(8,128)(2,1)S(1)}, u32[]{:S(2)}, u32[]{:S(2)}) %collective-permute-start.29) | collective-permute-done | bytes 327712 | tf_op jit(solution)/shard_map/ppermute | solution.py:148
  104.9 3.9 %collective-permute-start.30 = (bf16[80,2048]{1,0:T(8,128)(2,1)S(1)}, bf16[80,2048]{1,0:T(8,128)(2,1)S(1)}, u32[]{:S(2)}, u32[]{:S(2)}) collective-permute-start(bf16[80,2048]{1,0:T(8,128)(2,1)S(1)} %add_convert_fusion), channel_id=1, source_target_pairs={{0,8},{1,9},{2,10},{3,11},{4,12},{5,13},{6,14},{7,15},{8,0},{9,1},... | collective-permute-start | bytes 983048 | tf_op jit(solution)/shard_map/ppermute | solution.py:145
  109.0 10.6 %collective-permute-done.22.refs_0_ = bf16[80,2048]{1,0:T(8,128)(2,1)S(1)} collective-permute-done((bf16[80,2048]{1,0:T(8,128)(2,1)S(1)}, bf16[80,2048]{1,0:T(8,128)(2,1)S(1)}, u32[]{:S(2)}, u32[]{:S(2)}) %collective-permute-start.22) | collective-permute-done | bytes 327712 | tf_op jit(solution)/shard_map/ppermute | solution.py:145
  119.6 10.5 %collective-permute-done.30.refs_1_ = bf16[80,2048]{1,0:T(8,128)(2,1)S(1)} collective-permute-done((bf16[80,2048]{1,0:T(8,128)(2,1)S(1)}, bf16[80,2048]{1,0:T(8,128)(2,1)S(1)}, u32[]{:S(2)}, u32[]{:S(2)}) %collective-permute-start.30) | collective-permute-done | bytes 327712 | tf_op jit(solution)/shard_map/ppermute | solution.py:145
  130.9 1.6 %combine.3 = bf16[128,2048]{1,0:T(8,128)(2,1)} custom-call(s32[1]{0:T(128)} %bitcast.mine, s32[2,128]{1,0:T(2,128)S(1)} %bitcast.6, f32[2,128]{1,0:T(2,128)S(1)} %bitcast.8, bf16[80,2048]{1,0:T(8,128)(2,1)S(1)} %collective-permute-done.9.refs_0_, bf16[80,2048]{1,0:T(8,128)(2,1)S(1)} %add_convert_fusion.4.refs_1_, f32[128,2048]{1,0:T(8,128)S(1)} %combine.2.refs_2_), custom_call_target="tpu_custom_call" | custom-call | flops 83886080 | bytes 2097152 | tf_op jit(solution)/shard_map/combine/pallas_call | solution.py:230
  (61 shorter events, 17.0 us)
Async XLA Ops:
  1.8 7.3 %collective-permute-start.2 = (bf16[80,2048]{1,0:T(8,128)(2,1)S(1)}, bf16[80,2048]{1,0:T(8,128)(2,1)S(1)}, u32[]{:S(2)}, u32[]{:S(2)}) collective-permute-start(bf16[80,2048]{1,0:T(8,128)(2,1)S(1)} %get-tuple-element.29.refs_0_), channel_id=1, source_target_pairs={{0,1},{1,0},{2,3},{3,2},{4,5},{5,4},{6,7},{7,6},{8,9},{9,8},{10,11... | collective-permute-start | bytes 983048 | tf_op jit(solution)/shard_map/ppermute | solution.py:148
  2.3 13.3 %collective-permute-start = (bf16[80,2048]{1,0:T(8,128)(2,1)S(1)}, bf16[80,2048]{1,0:T(8,128)(2,1)S(1)}, u32[]{:S(2)}, u32[]{:S(2)}) collective-permute-start(bf16[80,2048]{1,0:T(8,128)(2,1)S(1)} %get-tuple-element.28), channel_id=1, source_target_pairs={{0,4},{1,5},{2,6},{3,7},{4,8},{5,9},{6,10},{7,11},{8,12},{9,13},{1... | collective-permute-start | bytes 983048 | tf_op jit(solution)/shard_map/ppermute | solution.py:145
  5.0 36.7 %collective-permute-start.4 = (bf16[80,2048]{1,0:T(8,128)(2,1)S(1)}, bf16[80,2048]{1,0:T(8,128)(2,1)S(1)}, u32[]{:S(2)}, u32[]{:S(2)}) collective-permute-start(bf16[80,2048]{1,0:T(8,128)(2,1)S(1)} %get-tuple-element.28), channel_id=1, source_target_pairs={{0,2},{1,3},{2,0},{3,1},{4,6},{5,7},{6,4},{7,5},{8,10},{9,11},{10,... | collective-permute-start | bytes 983048 | tf_op jit(solution)/shard_map/ppermute | solution.py:148
  6.5 17.4 %collective-permute-start.11 = (bf16[80,2048]{1,0:T(8,128)(2,1)S(1)}, bf16[80,2048]{1,0:T(8,128)(2,1)S(1)}, u32[]{:S(2)}, u32[]{:S(2)}) collective-permute-start(bf16[80,2048]{1,0:T(8,128)(2,1)S(1)} %get-tuple-element.29.refs_0_), channel_id=1, source_target_pairs={{0,2},{1,3},{2,0},{3,1},{4,6},{5,7},{6,4},{7,5},{8,10},{9,11},{10,... | collective-permute-start | bytes 983048 | tf_op jit(solution)/shard_map/ppermute | solution.py:148
  7.0 17.5 %collective-permute-start.15 = (bf16[80,2048]{1,0:T(8,128)(2,1)S(1)}, bf16[80,2048]{1,0:T(8,128)(2,1)S(1)}, u32[]{:S(2)}, u32[]{:S(2)}) collective-permute-start(bf16[80,2048]{1,0:T(8,128)(2,1)S(1)} %get-tuple-element.41), channel_id=1, source_target_pairs={{0,12},{1,13},{2,14},{3,15},{4,0},{5,1},{6,2},{7,3},{8,4},{9,5},{1... | collective-permute-start | bytes 983048 | tf_op jit(solution)/shard_map/ppermute | solution.py:145
  9.1 27.3 %collective-permute-start.23 = (bf16[80,2048]{1,0:T(8,128)(2,1)S(1)}, bf16[80,2048]{1,0:T(8,128)(2,1)S(1)}, u32[]{:S(2)}, u32[]{:S(2)}) collective-permute-start(bf16[80,2048]{1,0:T(8,128)(2,1)S(1)} %get-tuple-element.46), channel_id=1, source_target_pairs={{0,8},{1,9},{2,10},{3,11},{4,12},{5,13},{6,14},{7,15},{8,0},{9,1},... | collective-permute-start | bytes 983048 | tf_op jit(solution)/shard_map/ppermute | solution.py:145
  15.6 8.9 %collective-permute-start.1 = (bf16[80,2048]{1,0:T(8,128)(2,1)S(1)}, bf16[80,2048]{1,0:T(8,128)(2,1)S(1)}, u32[]{:S(2)}, u32[]{:S(2)}) collective-permute-start(bf16[80,2048]{1,0:T(8,128)(2,1)S(1)} %collective-permute-done.refs_0_), channel_id=1, source_target_pairs={{0,1},{1,0},{2,3},{3,2},{4,5},{5,4},{6,7},{7,6},{8,9},{9,8},{10,11... | collective-permute-start | bytes 983048 | tf_op jit(solution)/shard_map/ppermute | solution.py:148
  23.9 84.9 %collective-permute-start.10 = (bf16[80,2048]{1,0:T(8,128)(2,1)S(1)}, bf16[80,2048]{1,0:T(8,128)(2,1)S(1)}, u32[]{:S(2)}, u32[]{:S(2)}) collective-permute-start(bf16[80,2048]{1,0:T(8,128)(2,1)S(1)} %get-tuple-element.38), channel_id=1, source_target_pairs={{0,1},{1,0},{2,3},{3,2},{4,5},{5,4},{6,7},{7,6},{8,9},{9,8},{10,11... | collective-permute-start | bytes 983048 | tf_op jit(solution)/shard_map/ppermute | solution.py:148
  24.4 11.9 %collective-permute-start.12 = (bf16[80,2048]{1,0:T(8,128)(2,1)S(1)}, bf16[80,2048]{1,0:T(8,128)(2,1)S(1)}, u32[]{:S(2)}, u32[]{:S(2)}) collective-permute-start(bf16[80,2048]{1,0:T(8,128)(2,1)S(1)} %collective-permute-done.11.refs_0_), channel_id=1, source_target_pairs={{0,1},{1,0},{2,3},{3,2},{4,5},{5,4},{6,7},{7,6},{8,9},{9,8},{10,11... | collective-permute-start | bytes 983048 | tf_op jit(solution)/shard_map/ppermute | solution.py:148
  24.5 31.5 %collective-permute-start.18 = (bf16[80,2048]{1,0:T(8,128)(2,1)S(1)}, bf16[80,2048]{1,0:T(8,128)(2,1)S(1)}, u32[]{:S(2)}, u32[]{:S(2)}) collective-permute-start(bf16[80,2048]{1,0:T(8,128)(2,1)S(1)} %collective-permute-done.15.refs_0_), channel_id=1, source_target_pairs={{0,2},{1,3},{2,0},{3,1},{4,6},{5,7},{6,4},{7,5},{8,10},{9,11},{10,... | collective-permute-start | bytes 983048 | tf_op jit(solution)/shard_map/ppermute | solution.py:148
  36.4 5.6 %collective-permute-start.16 = (bf16[80,2048]{1,0:T(8,128)(2,1)S(1)}, bf16[80,2048]{1,0:T(8,128)(2,1)S(1)}, u32[]{:S(2)}, u32[]{:S(2)}) collective-permute-start(bf16[80,2048]{1,0:T(8,128)(2,1)S(1)} %collective-permute-done.15.refs_0_), channel_id=1, source_target_pairs={{0,1},{1,0},{2,3},{3,2},{4,5},{5,4},{6,7},{7,6},{8,9},{9,8},{10,11... | collective-permute-start | bytes 983048 | tf_op jit(solution)/shard_map/ppermute | solution.py:148
  36.4 25.4 %collective-permute-start.26 = (bf16[80,2048]{1,0:T(8,128)(2,1)S(1)}, bf16[80,2048]{1,0:T(8,128)(2,1)S(1)}, u32[]{:S(2)}, u32[]{:S(2)}) collective-permute-start(bf16[80,2048]{1,0:T(8,128)(2,1)S(1)} %collective-permute-done.23.refs_0_), channel_id=1, source_target_pairs={{0,2},{1,3},{2,0},{3,1},{4,6},{5,7},{6,4},{7,5},{8,10},{9,11},{10,... | collective-permute-start | bytes 983048 | tf_op jit(solution)/shard_map/ppermute | solution.py:148
  41.7 9.7 %collective-permute-start.24 = (bf16[80,2048]{1,0:T(8,128)(2,1)S(1)}, bf16[80,2048]{1,0:T(8,128)(2,1)S(1)}, u32[]{:S(2)}, u32[]{:S(2)}) collective-permute-start(bf16[80,2048]{1,0:T(8,128)(2,1)S(1)} %collective-permute-done.23.refs_0_), channel_id=1, source_target_pairs={{0,1},{1,0},{2,3},{3,2},{4,5},{5,4},{6,7},{7,6},{8,9},{9,8},{10,11... | collective-permute-start | bytes 983048 | tf_op jit(solution)/shard_map/ppermute | solution.py:148
  42.0 13.3 %collective-permute-start.5 = (bf16[80,2048]{1,0:T(8,128)(2,1)S(1)}, bf16[80,2048]{1,0:T(8,128)(2,1)S(1)}, u32[]{:S(2)}, u32[]{:S(2)}) collective-permute-start(bf16[80,2048]{1,0:T(8,128)(2,1)S(1)} %collective-permute-done.4), channel_id=1, source_target_pairs={{0,4},{1,5},{2,6},{3,7},{4,8},{5,9},{6,10},{7,11},{8,12},{9,13},{1... | collective-permute-start | bytes 983048 | tf_op jit(solution)/shard_map/ppermute | solution.py:145
  55.3 20.0 %collective-permute-start.3 = (bf16[80,2048]{1,0:T(8,128)(2,1)S(1)}, bf16[80,2048]{1,0:T(8,128)(2,1)S(1)}, u32[]{:S(2)}, u32[]{:S(2)}) collective-permute-start(bf16[80,2048]{1,0:T(8,128)(2,1)S(1)} %get-tuple-element.34), channel_id=1, source_target_pairs={{0,1},{1,0},{2,3},{3,2},{4,5},{5,4},{6,7},{7,6},{8,9},{9,8},{10,11... | collective-permute-start | bytes 983048 | tf_op jit(solution)/shard_map/ppermute | solution.py:148
  56.1 29.9 %collective-permute-start.17 = (bf16[80,2048]{1,0:T(8,128)(2,1)S(1)}, bf16[80,2048]{1,0:T(8,128)(2,1)S(1)}, u32[]{:S(2)}, u32[]{:S(2)}) collective-permute-start(bf16[80,2048]{1,0:T(8,128)(2,1)S(1)} %get-tuple-element.43), channel_id=1, source_target_pairs={{0,1},{1,0},{2,3},{3,2},{4,5},{5,4},{6,7},{7,6},{8,9},{9,8},{10,11... | collective-permute-start | bytes 983048 | tf_op jit(solution)/shard_map/ppermute | solution.py:148
  61.8 40.5 %collective-permute-start.25 = (bf16[80,2048]{1,0:T(8,128)(2,1)S(1)}, bf16[80,2048]{1,0:T(8,128)(2,1)S(1)}, u32[]{:S(2)}, u32[]{:S(2)}) collective-permute-start(bf16[80,2048]{1,0:T(8,128)(2,1)S(1)} %get-tuple-element.48), channel_id=1, source_target_pairs={{0,1},{1,0},{2,3},{3,2},{4,5},{5,4},{6,7},{7,6},{8,9},{9,8},{10,11... | collective-permute-start | bytes 983048 | tf_op jit(solution)/shard_map/ppermute | solution.py:148
  73.7 10.6 %collective-permute-start.8 = (bf16[80,2048]{1,0:T(8,128)(2,1)S(1)}, bf16[80,2048]{1,0:T(8,128)(2,1)S(1)}, u32[]{:S(2)}, u32[]{:S(2)}) collective-permute-start(bf16[80,2048]{1,0:T(8,128)(2,1)S(1)} %add_convert_fusion.7), channel_id=1, source_target_pairs={{0,2},{1,3},{2,0},{3,1},{4,6},{5,7},{6,4},{7,5},{8,10},{9,11},{10,... | collective-permute-start | bytes 983048 | tf_op jit(solution)/shard_map/ppermute | solution.py:148
  75.4 33.5 %collective-permute-start.14 = (bf16[80,2048]{1,0:T(8,128)(2,1)S(1)}, bf16[80,2048]{1,0:T(8,128)(2,1)S(1)}, u32[]{:S(2)}, u32[]{:S(2)}) collective-permute-start(bf16[80,2048]{1,0:T(8,128)(2,1)S(1)} %add_convert_fusion.5), channel_id=1, source_target_pairs={{0,2},{1,3},{2,0},{3,1},{4,6},{5,7},{6,4},{7,5},{8,10},{9,11},{10,... | collective-permute-start | bytes 983048 | tf_op jit(solution)/shard_map/ppermute | solution.py:148
  84.3 14.0 %collective-permute-start.21 = (bf16[80,2048]{1,0:T(8,128)(2,1)S(1)}, bf16[80,2048]{1,0:T(8,128)(2,1)S(1)}, u32[]{:S(2)}, u32[]{:S(2)}) collective-permute-start(bf16[80,2048]{1,0:T(8,128)(2,1)S(1)} %add_convert_fusion.3), channel_id=1, source_target_pairs={{0,2},{1,3},{2,0},{3,1},{4,6},{5,7},{6,4},{7,5},{8,10},{9,11},{10,... | collective-permute-start | bytes 983048 | tf_op jit(solution)/shard_map/ppermute | solution.py:148
  86.0 18.8 %collective-permute-start.29 = (bf16[80,2048]{1,0:T(8,128)(2,1)S(1)}, bf16[80,2048]{1,0:T(8,128)(2,1)S(1)}, u32[]{:S(2)}, u32[]{:S(2)}) collective-permute-start(bf16[80,2048]{1,0:T(8,128)(2,1)S(1)} %add_convert_fusion.1), channel_id=1, source_target_pairs={{0,2},{1,3},{2,0},{3,1},{4,6},{5,7},{6,4},{7,5},{8,10},{9,11},{10,... | collective-permute-start | bytes 983048 | tf_op jit(solution)/shard_map/ppermute | solution.py:148
  98.4 32.5 %collective-permute-start.9 = (bf16[80,2048]{1,0:T(8,128)(2,1)S(1)}, bf16[80,2048]{1,0:T(8,128)(2,1)S(1)}, u32[]{:S(2)}, u32[]{:S(2)}) collective-permute-start(bf16[80,2048]{1,0:T(8,128)(2,1)S(1)} %add_convert_fusion.6), channel_id=1, source_target_pairs={{0,12},{1,13},{2,14},{3,15},{4,0},{5,1},{6,2},{7,3},{8,4},{9,5},{1... | collective-permute-start | bytes 983048 | tf_op jit(solution)/shard_map/ppermute | solution.py:145
  102.3 17.3 %collective-permute-start.22 = (bf16[80,2048]{1,0:T(8,128)(2,1)S(1)}, bf16[80,2048]{1,0:T(8,128)(2,1)S(1)}, u32[]{:S(2)}, u32[]{:S(2)}) collective-permute-start(bf16[80,2048]{1,0:T(8,128)(2,1)S(1)} %add_convert_fusion.2), channel_id=1, source_target_pairs={{0,4},{1,5},{2,6},{3,7},{4,8},{5,9},{6,10},{7,11},{8,12},{9,13},{1... | collective-permute-start | bytes 983048 | tf_op jit(solution)/shard_map/ppermute | solution.py:145
  104.9 25.1 %collective-permute-start.30 = (bf16[80,2048]{1,0:T(8,128)(2,1)S(1)}, bf16[80,2048]{1,0:T(8,128)(2,1)S(1)}, u32[]{:S(2)}, u32[]{:S(2)}) collective-permute-start(bf16[80,2048]{1,0:T(8,128)(2,1)S(1)} %add_convert_fusion), channel_id=1, source_target_pairs={{0,8},{1,9},{2,10},{3,11},{4,12},{5,13},{6,14},{7,15},{8,0},{9,1},... | collective-permute-start | bytes 983048 | tf_op jit(solution)/shard_map/ppermute | solution.py:145
  (9 other events, 141.6 us)

commit v2 on v1

--- a/solution.py
+++ b/solution.py
@@ -53,22 +53,41 @@
         out[...] = jnp.dot(onehot, normed, preferred_element_type=jnp.float32).astype(jnp.bfloat16)
 
 
-def combine_kernel(experts, capacity, chosen, last, mine, ids, mix, *refs):
-    rets, refs = refs[: len(chosen)], refs[len(chosen) :]
-    total = refs[0][...] if last else None
-    out = refs[-1]
+def table(experts, capacity, mine, ids, mix, shift):
     tokens = ids.shape[1]
+    expert = lax.rem(mine[0] + shift, experts)
+    weight = jnp.zeros((1, tokens), jnp.float32)
+    for pick in range(TOP):
+        weight = weight + jnp.where(ids[pick : pick + 1] == expert, mix[pick : pick + 1], 0.0)
+    column = jnp.transpose(jnp.broadcast_to(weight, (tokens, tokens)))
+    return places(ids[...], expert, capacity), column
+
+
+def weighted(onehot, column, ret):
+    rows = lax.dot_general(
+        onehot, ret, (((0,), (0,)), ((), ())), preferred_element_type=jnp.float32
+    )
+    return column[:, 0:1] * rows
+
+
+def early_kernel(experts, capacity, chosen, late, mine, ids, mix, *refs):
+    rets, out, tables = refs[: len(chosen)], refs[len(chosen)], refs[len(chosen) + 1 :]
+    total = None
     for shift, ret in zip(chosen, rets):
-        expert = lax.rem(mine[0] + shift, experts)
-        onehot = places(ids[...], expert, capacity)
-        weight = jnp.zeros((1, tokens), jnp.float32)
-        for pick in range(TOP):
-            weight = weight + jnp.where(ids[pick : pick + 1] == expert, mix[pick : pick + 1], 0.0)
-        column = jnp.transpose(jnp.broadcast_to(weight, (tokens, tokens)))[:, 0:1]
-        rows = lax.dot_general(
-            onehot, ret[...], (((0,), (0,)), ((), ())), preferred_element_type=jnp.float32
-        )
-        total = column * rows if total is None else total + column * rows
+        part = weighted(*table(experts, capacity, mine, ids, mix, shift), ret[...])
+        total = part if total is None else total + part
+    out[...] = total
+    for k, shift in enumerate(late):
+        onehot, column = table(experts, capacity, mine, ids, mix, shift)
+        tables[2 * k][...] = onehot
+        tables[2 * k + 1][...] = column
+
+
+def final_kernel(count, *refs):
+    total, out = refs[0][...], refs[-1]
+    for k in range(count):
+        onehot, column, ret = (ref[...] for ref in refs[1 + 3 * k : 4 + 3 * k])
+        total = total + weighted(onehot, column, ret)
     out[...] = total.astype(out.dtype)
 
 
@@ -226,24 +245,30 @@
         total = add(part, got, got_far)
         rets[d] = across(total, experts - d) if d else total
 
-    def combine(chosen, dtype, *before):
-        return pl.pallas_call(
-            functools.partial(combine_kernel, experts, capacity, chosen, bool(before)),
-            out_shape=jax.ShapeDtypeStruct((tok_rows, width), dtype),
-            in_specs=[SMEM] + [VMEM] * (2 + len(chosen) + len(before)),
-            out_specs=VMEM,
-            compiler_params=pltpu.CompilerParams(vmem_limit_bytes=8 * 2**20),
-            cost_estimate=pl.CostEstimate(
-                flops=2 * len(chosen) * capacity * tok_rows * width,
-                bytes_accessed=8 * tok_rows * width,
-                transcendentals=0,
-            ),
-            name="combine",
-        )(mine, ids, mix, *(rets[d] for d in chosen), *before)
-
     late = LATE if experts == 4 else tuple(order[-1:])
-    early = combine(tuple(d for d in order if d not in late), jnp.float32)
-    return combine(late, jnp.bfloat16, early)
+    chosen = tuple(d for d in order if d not in late)
+    tables = [
+        jax.ShapeDtypeStruct((capacity, tok_rows), jnp.bfloat16),
+        jax.ShapeDtypeStruct((tok_rows, tok_rows), jnp.float32),
+    ]
+    params = pltpu.CompilerParams(vmem_limit_bytes=8 * 2**20)
+    total, *tables = pl.pallas_call(
+        functools.partial(early_kernel, experts, capacity, chosen, late),
+        out_shape=[jax.ShapeDtypeStruct((tok_rows, width), jnp.float32)] + tables * len(late),
+        in_specs=[SMEM] + [VMEM] * (2 + len(chosen)),
+        out_specs=[VMEM] * (1 + 2 * len(late)),
+        compiler_params=params,
+        name="combine",
+    )(mine, ids, mix, *(rets[d] for d in chosen))
+    last = [array for k, d in enumerate(late) for array in (*tables[2 * k : 2 * k + 2], rets[d])]
+    return pl.pallas_call(
+        functools.partial(final_kernel, len(late)),
+        out_shape=jax.ShapeDtypeStruct((tok_rows, width), jnp.bfloat16),
+        in_specs=[VMEM] * (1 + len(last)),
+        out_specs=VMEM,
+        compiler_params=params,
+        name="finish",
+    )(total, *last)
 
 
 def solution(mesh):

time: 133 us -> 131 us (0.985)
  starting transfers between devices: 33.2 us -> 26.3 us
  waiting for transfers between devices: 59 us -> 64.5 us
    ppermute x7, starting transfers between devices: 19.1 us -> 13.1 us  [across(): return lax.ppermute(array, 'ep', pairs)]
    ppermute x24, waiting for transfers between devices: 26.1 us -> 31.2 us  [inside(): return lax.ppermute(array, 'ep', [(i, i ^ flip) for i in range(n_dev)])]
where the time goes in v2:
time: 131 us
  waiting for transfers between devices  64.5 us (49%)
  Pallas kernels  38.9 us (30%)
  starting transfers between devices  26.3 us (20%)
    ppermute x7, waiting for transfers between devices, across(): return lax.ppermute(array, 'ep', pairs)  33.3 us
    ppermute x24, waiting for transfers between devices, inside(): return lax.ppermute(array, 'ep', [(i, i ^ flip) for i in range(n_dev)])  31.2 us
    pallas_call x4, Pallas kernels, local(): part_side, part_twin_side = ffn(side, twin_side, *weights)  15.4 us
    ppermute x24, starting transfers between devices, inside(): return lax.ppermute(array, 'ep', [(i, i ^ flip) for i in range(n_dev)])  13.2 us
    ppermute x7, starting transfers between devices, across(): return lax.ppermute(array, 'ep', pairs)  13.1 us
    pallas_call x3, Pallas kernels, local(): part, part_twin = ffn(own, twin, *weights)  11.3 us
    pallas_call x1, Pallas kernels, local(): part, part_twin, *weights = first_ffn(own, twin, *kept)  8.26 us
  transfers between devices with their start and end apart: 31, of which 10 were waited for; matrix products, arithmetic and copies ran while one was open for 1% of the time, Pallas kernels for 27%

profile of v2, /device:TPU:0, one launch (start us, length us, event | category | flops | bytes accessed | tf_op | source)
XLA Modules:
  0.0 130.8 jit_solution(16820188398171409086)
XLA Ops:
  0.0 1.8 %route.1 = (bf16[80,2048]{1,0:T(8,128)(2,1)S(1)}, bf16[80,2048]{1,0:T(8,128)(2,1)S(1)}, bf16[80,2048]{1,0:T(8,128)(2,1)S(1)}, bf16[80,2048]{1,0:T(8,128)(2,1)S(1)}) custom-call(s32[1]{0:T(128)} %bitcast.mine, s32[2,128]{1,0:T(2,128)} %bitcast.4, bf16[128,2048]{1,0:T(8,128)(2,1)} %refs_1_.1, f32[1,2048]{1,0:T(1,128)} %bitcast.7), custom_call_target="tpu_custom_call" | custom-call | flops 167772160 | bytes 1048576 | tf_op jit(solution)/shard_map/route/pallas_call | solution.py:173
  2.3 2.6 %collective-permute-start.27 = (bf16[80,2048]{1,0:T(8,128)(2,1)S(1)}, bf16[80,2048]{1,0:T(8,128)(2,1)S(1)}, u32[]{:S(2)}, u32[]{:S(2)}) collective-permute-start(bf16[80,2048]{1,0:T(8,128)(2,1)S(1)} %get-tuple-element.34.refs_0_), channel_id=1, source_target_pairs={{0,2},{1,3},{2,0},{3,1},{4,6},{5,7},{6,4},{7,5},{8,10},{9,11},{10,... | collective-permute-start | bytes 983048 | tf_op jit(solution)/shard_map/ppermute | solution.py:167
  4.9 1.6 %collective-permute-start.17 = (bf16[80,2048]{1,0:T(8,128)(2,1)S(1)}, bf16[80,2048]{1,0:T(8,128)(2,1)S(1)}, u32[]{:S(2)}, u32[]{:S(2)}) collective-permute-start(bf16[80,2048]{1,0:T(8,128)(2,1)S(1)} %get-tuple-element.50), channel_id=1, source_target_pairs={{0,4},{1,5},{2,6},{3,7},{4,8},{5,9},{6,10},{7,11},{8,12},{9,13},{1... | collective-permute-start | bytes 983048 | tf_op jit(solution)/shard_map/ppermute | solution.py:164
  7.0 2.6 %collective-permute-start.9 = (bf16[80,2048]{1,0:T(8,128)(2,1)S(1)}, bf16[80,2048]{1,0:T(8,128)(2,1)S(1)}, u32[]{:S(2)}, u32[]{:S(2)}) collective-permute-start(bf16[80,2048]{1,0:T(8,128)(2,1)S(1)} %get-tuple-element.42), channel_id=1, source_target_pairs={{0,8},{1,9},{2,10},{3,11},{4,12},{5,13},{6,14},{7,15},{8,0},{9,1},... | collective-permute-start | bytes 983048 | tf_op jit(solution)/shard_map/ppermute | solution.py:164
  10.9 2.5 %collective-permute-done.27.refs_0_ = bf16[80,2048]{1,0:T(8,128)(2,1)S(1)} collective-permute-done((bf16[80,2048]{1,0:T(8,128)(2,1)S(1)}, bf16[80,2048]{1,0:T(8,128)(2,1)S(1)}, u32[]{:S(2)}, u32[]{:S(2)}) %collective-permute-start.27) | collective-permute-done | bytes 327712 | tf_op jit(solution)/shard_map/ppermute | solution.py:167
  13.5 8.3 %experts.8 = (bf16[80,2048]{1,0:T(8,128)(2,1)S(1)}, bf16[80,2048]{1,0:T(8,128)(2,1)S(1)}, bf16[2048,1792]{1,0:T(8,128)(2,1)S(1)}, bf16[2048,1792]{1,0:T(8,128)(2,1)S(1)}, bf16[1792,2048]{1,0:T(8,128)(2,1)S(1)}) custom-call(bf16[80,2048]{1,0:T(8,128)(2,1)S(1)} %get-tuple-element.34.refs_0_, bf16[80,2048]{1,0:T(8,128)(2,1)S(1)} %collective-permute-done.2.refs_1_, ...), custom_call_target="tpu_custom_call" | custom-call | flops 3523215360 | bytes 22020096 | tf_op jit(solution)/shard_map/experts/pallas_call | solution.py:237
  22.3 8.4 %collective-permute-done.9.refs_0_ = bf16[80,2048]{1,0:T(8,128)(2,1)S(1)} collective-permute-done((bf16[80,2048]{1,0:T(8,128)(2,1)S(1)}, bf16[80,2048]{1,0:T(8,128)(2,1)S(1)}, u32[]{:S(2)}, u32[]{:S(2)}) %collective-permute-start.9) | collective-permute-done | bytes 327712 | tf_op jit(solution)/shard_map/ppermute | solution.py:164
  31.2 3.8 %experts.15 = (bf16[80,2048]{1,0:T(8,128)(2,1)S(1)}, bf16[80,2048]{1,0:T(8,128)(2,1)S(1)}) custom-call(bf16[80,2048]{1,0:T(8,128)(2,1)S(1)} %collective-permute-done.27.refs_0_, bf16[80,2048]{1,0:T(8,128)(2,1)S(1)} %collective-permute-done.28.refs_1_, bf16[2048,1792]{1,0:T(8,128)(2,1)S(1)} %get-tuple-element.35.refs_2_, ...), custom_call_target="tpu_custom_call" | custom-call | flops 3523215360 | bytes 22020096 | tf_op jit(solution)/shard_map/experts/pallas_call | solution.py:240
  35.6 3.8 %experts.13 = (bf16[80,2048]{1,0:T(8,128)(2,1)S(1)}, bf16[80,2048]{1,0:T(8,128)(2,1)S(1)}) custom-call(bf16[80,2048]{1,0:T(8,128)(2,1)S(1)} %collective-permute-done.17.refs_0_, bf16[80,2048]{1,0:T(8,128)(2,1)S(1)} %collective-permute-done.18.refs_1_, bf16[2048,1792]{1,0:T(8,128)(2,1)S(1)} %get-tuple-element.35.refs_2_, ...), custom_call_target="tpu_custom_call" | custom-call | flops 3523215360 | bytes 22020096 | tf_op jit(solution)/shard_map/experts/pallas_call | solution.py:239
  39.4 1.6 %collective-permute-start.4 = (bf16[80,2048]{1,0:T(8,128)(2,1)S(1)}, bf16[80,2048]{1,0:T(8,128)(2,1)S(1)}, u32[]{:S(2)}, u32[]{:S(2)}) collective-permute-start(bf16[80,2048]{1,0:T(8,128)(2,1)S(1)} %collective-permute-done.refs_0_), channel_id=1, source_target_pairs={{0,2},{1,3},{2,0},{3,1},{4,6},{5,7},{6,4},{7,5},{8,10},{9,11},{10,... | collective-permute-start | bytes 983048 | tf_op jit(solution)/shard_map/ppermute | solution.py:167
  41.0 5.7 %collective-permute-start.21 = (bf16[80,2048]{1,0:T(8,128)(2,1)S(1)}, bf16[80,2048]{1,0:T(8,128)(2,1)S(1)}, u32[]{:S(2)}, u32[]{:S(2)}) collective-permute-start(bf16[80,2048]{1,0:T(8,128)(2,1)S(1)} %collective-permute-done.20), channel_id=1, source_target_pairs={{0,4},{1,5},{2,6},{3,7},{4,8},{5,9},{6,10},{7,11},{8,12},{9,13},{1... | collective-permute-start | bytes 983048 | tf_op jit(solution)/shard_map/ppermute | solution.py:164
  46.7 3.8 %experts.11 = (bf16[80,2048]{1,0:T(8,128)(2,1)S(1)}, bf16[80,2048]{1,0:T(8,128)(2,1)S(1)}) custom-call(bf16[80,2048]{1,0:T(8,128)(2,1)S(1)} %collective-permute-done.9.refs_0_, bf16[80,2048]{1,0:T(8,128)(2,1)S(1)} %collective-permute-done.10.refs_1_, bf16[2048,1792]{1,0:T(8,128)(2,1)S(1)} %get-tuple-element.35.refs_2_, ...), custom_call_target="tpu_custom_call" | custom-call | flops 3523215360 | bytes 22020096 | tf_op jit(solution)/shard_map/experts/pallas_call | solution.py:239
  50.6 3.8 %experts.9 = (bf16[80,2048]{1,0:T(8,128)(2,1)S(1)}, bf16[80,2048]{1,0:T(8,128)(2,1)S(1)}) custom-call(bf16[80,2048]{1,0:T(8,128)(2,1)S(1)} %collective-permute-done.refs_0_, bf16[80,2048]{1,0:T(8,128)(2,1)S(1)} %collective-permute-done.1.refs_1_, bf16[2048,1792]{1,0:T(8,128)(2,1)S(1)} %get-tuple-element.35.refs_2_, ...), custom_call_target="tpu_custom_call" | custom-call | flops 3523215360 | bytes 22020096 | tf_op jit(solution)/shard_map/experts/pallas_call | solution.py:239
  54.4 3.2 %collective-permute-done.21.refs_0_ = bf16[80,2048]{1,0:T(8,128)(2,1)S(1)} collective-permute-done((bf16[80,2048]{1,0:T(8,128)(2,1)S(1)}, bf16[80,2048]{1,0:T(8,128)(2,1)S(1)}, u32[]{:S(2)}, u32[]{:S(2)}) %collective-permute-start.21) | collective-permute-done | bytes 327712 | tf_op jit(solution)/shard_map/ppermute | solution.py:164
  59.8 3.8 %experts.14 = (bf16[80,2048]{1,0:T(8,128)(2,1)S(1)}, bf16[80,2048]{1,0:T(8,128)(2,1)S(1)}) custom-call(bf16[80,2048]{1,0:T(8,128)(2,1)S(1)} %collective-permute-done.21.refs_0_, bf16[80,2048]{1,0:T(8,128)(2,1)S(1)} %collective-permute-done.22.refs_1_, bf16[2048,1792]{1,0:T(8,128)(2,1)S(1)} %get-tuple-element.35.refs_2_, ...), custom_call_target="tpu_custom_call" | custom-call | flops 3523215360 | bytes 22020096 | tf_op jit(solution)/shard_map/experts/pallas_call | solution.py:240
  64.2 4.0 %experts.12 = (bf16[80,2048]{1,0:T(8,128)(2,1)S(1)}, bf16[80,2048]{1,0:T(8,128)(2,1)S(1)}) custom-call(bf16[80,2048]{1,0:T(8,128)(2,1)S(1)} %collective-permute-done.12.refs_0_, bf16[80,2048]{1,0:T(8,128)(2,1)S(1)} %collective-permute-done.13.refs_1_, bf16[2048,1792]{1,0:T(8,128)(2,1)S(1)} %get-tuple-element.35.refs_2_, ...), custom_call_target="tpu_custom_call" | custom-call | flops 3523215360 | bytes 22020096 | tf_op jit(solution)/shard_map/experts/pallas_call | solution.py:240
  68.7 3.8 %experts.10 = (bf16[80,2048]{1,0:T(8,128)(2,1)S(1)}, bf16[80,2048]{1,0:T(8,128)(2,1)S(1)}) custom-call(bf16[80,2048]{1,0:T(8,128)(2,1)S(1)} %collective-permute-done.4.refs_0_, bf16[80,2048]{1,0:T(8,128)(2,1)S(1)} %collective-permute-done.5.refs_1_, bf16[2048,1792]{1,0:T(8,128)(2,1)S(1)} %get-tuple-element.35.refs_2_, ...), custom_call_target="tpu_custom_call" | custom-call | flops 3523215360 | bytes 22020096 | tf_op jit(solution)/shard_map/experts/pallas_call | solution.py:240
  76.5 1.6 %collective-permute-start.30 = (bf16[80,2048]{1,0:T(8,128)(2,1)S(1)}, bf16[80,2048]{1,0:T(8,128)(2,1)S(1)}, u32[]{:S(2)}, u32[]{:S(2)}) collective-permute-start(bf16[80,2048]{1,0:T(8,128)(2,1)S(1)} %add_convert_fusion.1), channel_id=1, source_target_pairs={{0,2},{1,3},{2,0},{3,1},{4,6},{5,7},{6,4},{7,5},{8,10},{9,11},{10,... | collective-permute-start | bytes 983048 | tf_op jit(solution)/shard_map/ppermute | solution.py:167
  78.0 8.4 %collective-permute-done.24 = bf16[80,2048]{1,0:T(8,128)(2,1)S(1)} collective-permute-done((bf16[80,2048]{1,0:T(8,128)(2,1)S(1)}, bf16[80,2048]{1,0:T(8,128)(2,1)S(1)}, u32[]{:S(2)}, u32[]{:S(2)}) %collective-permute-start.24) | collective-permute-done | bytes 327712 | tf_op jit(solution)/shard_map/ppermute | solution.py:167
  87.1 1.6 %collective-permute-start.7 = (bf16[80,2048]{1,0:T(8,128)(2,1)S(1)}, bf16[80,2048]{1,0:T(8,128)(2,1)S(1)}, u32[]{:S(2)}, u32[]{:S(2)}) collective-permute-start(bf16[80,2048]{1,0:T(8,128)(2,1)S(1)} %add_convert_fusion.7), channel_id=1, source_target_pairs={{0,2},{1,3},{2,0},{3,1},{4,6},{5,7},{6,4},{7,5},{8,10},{9,11},{10,... | collective-permute-start | bytes 983048 | tf_op jit(solution)/shard_map/ppermute | solution.py:167
  88.7 11.8 %collective-permute-done.15 = bf16[80,2048]{1,0:T(8,128)(2,1)S(1)} collective-permute-done((bf16[80,2048]{1,0:T(8,128)(2,1)S(1)}, bf16[80,2048]{1,0:T(8,128)(2,1)S(1)}, u32[]{:S(2)}, u32[]{:S(2)}) %collective-permute-start.15) | collective-permute-done | bytes 327712 | tf_op jit(solution)/shard_map/ppermute | solution.py:167
  100.5 1.7 %collective-permute-start.25 = (bf16[80,2048]{1,0:T(8,128)(2,1)S(1)}, bf16[80,2048]{1,0:T(8,128)(2,1)S(1)}, u32[]{:S(2)}, u32[]{:S(2)}) collective-permute-start(bf16[80,2048]{1,0:T(8,128)(2,1)S(1)} %add_convert_fusion.2), channel_id=1, source_target_pairs={{0,12},{1,13},{2,14},{3,15},{4,0},{5,1},{6,2},{7,3},{8,4},{9,5},{1... | collective-permute-start | bytes 983048 | tf_op jit(solution)/shard_map/ppermute | solution.py:164
  102.4 4.2 %collective-permute-done.7 = bf16[80,2048]{1,0:T(8,128)(2,1)S(1)} collective-permute-done((bf16[80,2048]{1,0:T(8,128)(2,1)S(1)}, bf16[80,2048]{1,0:T(8,128)(2,1)S(1)}, u32[]{:S(2)}, u32[]{:S(2)}) %collective-permute-start.7) | collective-permute-done | bytes 327712 | tf_op jit(solution)/shard_map/ppermute | solution.py:167
  107.0 21.6 %collective-permute-done.16.refs_1_ = bf16[80,2048]{1,0:T(8,128)(2,1)S(1)} collective-permute-done((bf16[80,2048]{1,0:T(8,128)(2,1)S(1)}, bf16[80,2048]{1,0:T(8,128)(2,1)S(1)}, u32[]{:S(2)}, u32[]{:S(2)}) %collective-permute-start.16) | collective-permute-done | bytes 327712 | tf_op jit(solution)/shard_map/ppermute | solution.py:164
  (61 shorter events, 14.7 us)
Async XLA Ops:
  1.8 7.8 %collective-permute-start.2 = (bf16[80,2048]{1,0:T(8,128)(2,1)S(1)}, bf16[80,2048]{1,0:T(8,128)(2,1)S(1)}, u32[]{:S(2)}, u32[]{:S(2)}) collective-permute-start(bf16[80,2048]{1,0:T(8,128)(2,1)S(1)} %get-tuple-element.34.refs_0_), channel_id=1, source_target_pairs={{0,1},{1,0},{2,3},{3,2},{4,5},{5,4},{6,7},{7,6},{8,9},{9,8},{10,11... | collective-permute-start | bytes 983048 | tf_op jit(solution)/shard_map/ppermute | solution.py:167
  2.3 11.1 %collective-permute-start.27 = (bf16[80,2048]{1,0:T(8,128)(2,1)S(1)}, bf16[80,2048]{1,0:T(8,128)(2,1)S(1)}, u32[]{:S(2)}, u32[]{:S(2)}) collective-permute-start(bf16[80,2048]{1,0:T(8,128)(2,1)S(1)} %get-tuple-element.34.refs_0_), channel_id=1, source_target_pairs={{0,2},{1,3},{2,0},{3,1},{4,6},{5,7},{6,4},{7,5},{8,10},{9,11},{10,... | collective-permute-start | bytes 983048 | tf_op jit(solution)/shard_map/ppermute | solution.py:167
  4.9 16.8 %collective-permute-start.17 = (bf16[80,2048]{1,0:T(8,128)(2,1)S(1)}, bf16[80,2048]{1,0:T(8,128)(2,1)S(1)}, u32[]{:S(2)}, u32[]{:S(2)}) collective-permute-start(bf16[80,2048]{1,0:T(8,128)(2,1)S(1)} %get-tuple-element.50), channel_id=1, source_target_pairs={{0,4},{1,5},{2,6},{3,7},{4,8},{5,9},{6,10},{7,11},{8,12},{9,13},{1... | collective-permute-start | bytes 983048 | tf_op jit(solution)/shard_map/ppermute | solution.py:164
  6.5 32.9 %collective-permute-start.20 = (bf16[80,2048]{1,0:T(8,128)(2,1)S(1)}, bf16[80,2048]{1,0:T(8,128)(2,1)S(1)}, u32[]{:S(2)}, u32[]{:S(2)}) collective-permute-start(bf16[80,2048]{1,0:T(8,128)(2,1)S(1)} %get-tuple-element.50), channel_id=1, source_target_pairs={{0,2},{1,3},{2,0},{3,1},{4,6},{5,7},{6,4},{7,5},{8,10},{9,11},{10,... | collective-permute-start | bytes 983048 | tf_op jit(solution)/shard_map/ppermute | solution.py:167
  7.0 23.7 %collective-permute-start.9 = (bf16[80,2048]{1,0:T(8,128)(2,1)S(1)}, bf16[80,2048]{1,0:T(8,128)(2,1)S(1)}, u32[]{:S(2)}, u32[]{:S(2)}) collective-permute-start(bf16[80,2048]{1,0:T(8,128)(2,1)S(1)} %get-tuple-element.42), channel_id=1, source_target_pairs={{0,8},{1,9},{2,10},{3,11},{4,12},{5,13},{6,14},{7,15},{8,0},{9,1},... | collective-permute-start | bytes 983048 | tf_op jit(solution)/shard_map/ppermute | solution.py:164
  9.6 25.4 %collective-permute-start = (bf16[80,2048]{1,0:T(8,128)(2,1)S(1)}, bf16[80,2048]{1,0:T(8,128)(2,1)S(1)}, u32[]{:S(2)}, u32[]{:S(2)}) collective-permute-start(bf16[80,2048]{1,0:T(8,128)(2,1)S(1)} %get-tuple-element.33), channel_id=1, source_target_pairs={{0,12},{1,13},{2,14},{3,15},{4,0},{5,1},{6,2},{7,3},{8,4},{9,5},{1... | collective-permute-start | bytes 983048 | tf_op jit(solution)/shard_map/ppermute | solution.py:164
  13.5 17.2 %collective-permute-start.28 = (bf16[80,2048]{1,0:T(8,128)(2,1)S(1)}, bf16[80,2048]{1,0:T(8,128)(2,1)S(1)}, u32[]{:S(2)}, u32[]{:S(2)}) collective-permute-start(bf16[80,2048]{1,0:T(8,128)(2,1)S(1)} %collective-permute-done.27.refs_0_), channel_id=1, source_target_pairs={{0,1},{1,0},{2,3},{3,2},{4,5},{5,4},{6,7},{7,6},{8,9},{9,8},{10,11... | collective-permute-start | bytes 983048 | tf_op jit(solution)/shard_map/ppermute | solution.py:167
  21.8 85.1 %collective-permute-start.26 = (bf16[80,2048]{1,0:T(8,128)(2,1)S(1)}, bf16[80,2048]{1,0:T(8,128)(2,1)S(1)}, u32[]{:S(2)}, u32[]{:S(2)}) collective-permute-start(bf16[80,2048]{1,0:T(8,128)(2,1)S(1)} %get-tuple-element.58), channel_id=1, source_target_pairs={{0,1},{1,0},{2,3},{3,2},{4,5},{5,4},{6,7},{7,6},{8,9},{9,8},{10,11... | collective-permute-start | bytes 983048 | tf_op jit(solution)/shard_map/ppermute | solution.py:167
  30.7 10.3 %collective-permute-start.10 = (bf16[80,2048]{1,0:T(8,128)(2,1)S(1)}, bf16[80,2048]{1,0:T(8,128)(2,1)S(1)}, u32[]{:S(2)}, u32[]{:S(2)}) collective-permute-start(bf16[80,2048]{1,0:T(8,128)(2,1)S(1)} %collective-permute-done.9.refs_0_), channel_id=1, source_target_pairs={{0,1},{1,0},{2,3},{3,2},{4,5},{5,4},{6,7},{7,6},{8,9},{9,8},{10,11... | collective-permute-start | bytes 983048 | tf_op jit(solution)/shard_map/ppermute | solution.py:167
  35.0 23.2 %collective-permute-start.12 = (bf16[80,2048]{1,0:T(8,128)(2,1)S(1)}, bf16[80,2048]{1,0:T(8,128)(2,1)S(1)}, u32[]{:S(2)}, u32[]{:S(2)}) collective-permute-start(bf16[80,2048]{1,0:T(8,128)(2,1)S(1)} %collective-permute-done.9.refs_0_), channel_id=1, source_target_pairs={{0,2},{1,3},{2,0},{3,1},{4,6},{5,7},{6,4},{7,5},{8,10},{9,11},{10,... | collective-permute-start | bytes 983048 | tf_op jit(solution)/shard_map/ppermute | solution.py:167
  35.6 14.9 %collective-permute-start.1 = (bf16[80,2048]{1,0:T(8,128)(2,1)S(1)}, bf16[80,2048]{1,0:T(8,128)(2,1)S(1)}, u32[]{:S(2)}, u32[]{:S(2)}) collective-permute-start(bf16[80,2048]{1,0:T(8,128)(2,1)S(1)} %collective-permute-done.refs_0_), channel_id=1, source_target_pairs={{0,1},{1,0},{2,3},{3,2},{4,5},{5,4},{6,7},{7,6},{8,9},{9,8},{10,11... | collective-permute-start | bytes 983048 | tf_op jit(solution)/shard_map/ppermute | solution.py:167
  39.4 24.2 %collective-permute-start.4 = (bf16[80,2048]{1,0:T(8,128)(2,1)S(1)}, bf16[80,2048]{1,0:T(8,128)(2,1)S(1)}, u32[]{:S(2)}, u32[]{:S(2)}) collective-permute-start(bf16[80,2048]{1,0:T(8,128)(2,1)S(1)} %collective-permute-done.refs_0_), channel_id=1, source_target_pairs={{0,2},{1,3},{2,0},{3,1},{4,6},{5,7},{6,4},{7,5},{8,10},{9,11},{10,... | collective-permute-start | bytes 983048 | tf_op jit(solution)/shard_map/ppermute | solution.py:167
  41.0 16.6 %collective-permute-start.21 = (bf16[80,2048]{1,0:T(8,128)(2,1)S(1)}, bf16[80,2048]{1,0:T(8,128)(2,1)S(1)}, u32[]{:S(2)}, u32[]{:S(2)}) collective-permute-start(bf16[80,2048]{1,0:T(8,128)(2,1)S(1)} %collective-permute-done.20), channel_id=1, source_target_pairs={{0,4},{1,5},{2,6},{3,7},{4,8},{5,9},{6,10},{7,11},{8,12},{9,13},{1... | collective-permute-start | bytes 983048 | tf_op jit(solution)/shard_map/ppermute | solution.py:164
  50.5 7.1 %collective-permute-start.29 = (bf16[80,2048]{1,0:T(8,128)(2,1)S(1)}, bf16[80,2048]{1,0:T(8,128)(2,1)S(1)}, u32[]{:S(2)}, u32[]{:S(2)}) collective-permute-start(bf16[80,2048]{1,0:T(8,128)(2,1)S(1)} %get-tuple-element.60), channel_id=1, source_target_pairs={{0,1},{1,0},{2,3},{3,2},{4,5},{5,4},{6,7},{7,6},{8,9},{9,8},{10,11... | collective-permute-start | bytes 983048 | tf_op jit(solution)/shard_map/ppermute | solution.py:167
  57.6 18.9 %collective-permute-start.19 = (bf16[80,2048]{1,0:T(8,128)(2,1)S(1)}, bf16[80,2048]{1,0:T(8,128)(2,1)S(1)}, u32[]{:S(2)}, u32[]{:S(2)}) collective-permute-start(bf16[80,2048]{1,0:T(8,128)(2,1)S(1)} %get-tuple-element.52), channel_id=1, source_target_pairs={{0,1},{1,0},{2,3},{3,2},{4,5},{5,4},{6,7},{7,6},{8,9},{9,8},{10,11... | collective-permute-start | bytes 983048 | tf_op jit(solution)/shard_map/ppermute | solution.py:167
  58.2 28.9 %collective-permute-start.11 = (bf16[80,2048]{1,0:T(8,128)(2,1)S(1)}, bf16[80,2048]{1,0:T(8,128)(2,1)S(1)}, u32[]{:S(2)}, u32[]{:S(2)}) collective-permute-start(bf16[80,2048]{1,0:T(8,128)(2,1)S(1)} %get-tuple-element.44), channel_id=1, source_target_pairs={{0,1},{1,0},{2,3},{3,2},{4,5},{5,4},{6,7},{7,6},{8,9},{9,8},{10,11... | collective-permute-start | bytes 983048 | tf_op jit(solution)/shard_map/ppermute | solution.py:167
  63.6 38.7 %collective-permute-start.3 = (bf16[80,2048]{1,0:T(8,128)(2,1)S(1)}, bf16[80,2048]{1,0:T(8,128)(2,1)S(1)}, u32[]{:S(2)}, u32[]{:S(2)}) collective-permute-start(bf16[80,2048]{1,0:T(8,128)(2,1)S(1)} %get-tuple-element.39), channel_id=1, source_target_pairs={{0,1},{1,0},{2,3},{3,2},{4,5},{5,4},{6,7},{7,6},{8,9},{9,8},{10,11... | collective-permute-start | bytes 983048 | tf_op jit(solution)/shard_map/ppermute | solution.py:167
  75.9 10.6 %collective-permute-start.24 = (bf16[80,2048]{1,0:T(8,128)(2,1)S(1)}, bf16[80,2048]{1,0:T(8,128)(2,1)S(1)}, u32[]{:S(2)}, u32[]{:S(2)}) collective-permute-start(bf16[80,2048]{1,0:T(8,128)(2,1)S(1)} %add_convert_fusion.3), channel_id=1, source_target_pairs={{0,2},{1,3},{2,0},{3,1},{4,6},{5,7},{6,4},{7,5},{8,10},{9,11},{10,... | collective-permute-start | bytes 983048 | tf_op jit(solution)/shard_map/ppermute | solution.py:167
  76.5 30.4 %collective-permute-start.30 = (bf16[80,2048]{1,0:T(8,128)(2,1)S(1)}, bf16[80,2048]{1,0:T(8,128)(2,1)S(1)}, u32[]{:S(2)}, u32[]{:S(2)}) collective-permute-start(bf16[80,2048]{1,0:T(8,128)(2,1)S(1)} %add_convert_fusion.1), channel_id=1, source_target_pairs={{0,2},{1,3},{2,0},{3,1},{4,6},{5,7},{6,4},{7,5},{8,10},{9,11},{10,... | collective-permute-start | bytes 983048 | tf_op jit(solution)/shard_map/ppermute | solution.py:167
  86.4 14.0 %collective-permute-start.15 = (bf16[80,2048]{1,0:T(8,128)(2,1)S(1)}, bf16[80,2048]{1,0:T(8,128)(2,1)S(1)}, u32[]{:S(2)}, u32[]{:S(2)}) collective-permute-start(bf16[80,2048]{1,0:T(8,128)(2,1)S(1)} %add_convert_fusion.5), channel_id=1, source_target_pairs={{0,2},{1,3},{2,0},{3,1},{4,6},{5,7},{6,4},{7,5},{8,10},{9,11},{10,... | collective-permute-start | bytes 983048 | tf_op jit(solution)/shard_map/ppermute | solution.py:167
  87.1 19.6 %collective-permute-start.7 = (bf16[80,2048]{1,0:T(8,128)(2,1)S(1)}, bf16[80,2048]{1,0:T(8,128)(2,1)S(1)}, u32[]{:S(2)}, u32[]{:S(2)}) collective-permute-start(bf16[80,2048]{1,0:T(8,128)(2,1)S(1)} %add_convert_fusion.7), channel_id=1, source_target_pairs={{0,2},{1,3},{2,0},{3,1},{4,6},{5,7},{6,4},{7,5},{8,10},{9,11},{10,... | collective-permute-start | bytes 983048 | tf_op jit(solution)/shard_map/ppermute | solution.py:167
  100.5 29.1 %collective-permute-start.25 = (bf16[80,2048]{1,0:T(8,128)(2,1)S(1)}, bf16[80,2048]{1,0:T(8,128)(2,1)S(1)}, u32[]{:S(2)}, u32[]{:S(2)}) collective-permute-start(bf16[80,2048]{1,0:T(8,128)(2,1)S(1)} %add_convert_fusion.2), channel_id=1, source_target_pairs={{0,12},{1,13},{2,14},{3,15},{4,0},{5,1},{6,2},{7,3},{8,4},{9,5},{1... | collective-permute-start | bytes 983048 | tf_op jit(solution)/shard_map/ppermute | solution.py:164
  102.4 26.3 %collective-permute-start.16 = (bf16[80,2048]{1,0:T(8,128)(2,1)S(1)}, bf16[80,2048]{1,0:T(8,128)(2,1)S(1)}, u32[]{:S(2)}, u32[]{:S(2)}) collective-permute-start(bf16[80,2048]{1,0:T(8,128)(2,1)S(1)} %add_convert_fusion.4), channel_id=1, source_target_pairs={{0,8},{1,9},{2,10},{3,11},{4,12},{5,13},{6,14},{7,15},{8,0},{9,1},... | collective-permute-start | bytes 983048 | tf_op jit(solution)/shard_map/ppermute | solution.py:164
  106.8 21.9 %collective-permute-start.8 = (bf16[80,2048]{1,0:T(8,128)(2,1)S(1)}, bf16[80,2048]{1,0:T(8,128)(2,1)S(1)}, u32[]{:S(2)}, u32[]{:S(2)}) collective-permute-start(bf16[80,2048]{1,0:T(8,128)(2,1)S(1)} %add_convert_fusion.6), channel_id=1, source_target_pairs={{0,4},{1,5},{2,6},{3,7},{4,8},{5,9},{6,10},{7,11},{8,12},{9,13},{1... | collective-permute-start | bytes 983048 | tf_op jit(solution)/shard_map/ppermute | solution.py:164
  (9 other events, 135.4 us)
